TPU v7x, 512 devices: a whole 4x8x8 slice. The times are simulated.
512 devices in a mesh: sp: 64 (over z, y), fs: 4 (over x), tp: 2 (over core).
Axes of the slice: x: 4, y: 8, z: 8, core: 2. Of those that a mesh axis runs over, the one named last changes fastest.
Arguments:
- tokens: bfloat16 [4, 16384, 2048], P('fs', 'sp', 'tp'), may hold values from -6 to 6
- norm_gain: float32 [2048], replicated, may hold values from 0.1 to 1.9
- ret_query: bfloat16 [2048, 1024], P('sp', 'tp'), may hold values from -0.125 to 0.125
- ret_key: bfloat16 [2048, 1024], P('sp', 'tp'), may hold values from -0.125 to 0.125
- ret_value: bfloat16 [2048, 1024], P('sp', 'tp'), may hold values from -0.125 to 0.125
- att_query: bfloat16 [2048, 1024], P('sp', 'tp'), may hold values from -0.125 to 0.125
- att_key: bfloat16 [2048, 256], P('sp', 'tp'), may hold values from -0.125 to 0.125
- att_value: bfloat16 [2048, 256], P('sp', 'tp'), may hold values from -0.125 to 0.125
- log_decay: float32 [4, 4, 16384], P('fs', 'tp', 'sp'), may hold values from -1 to 0
- start_state: float32 [4, 4, 256, 256], P('fs', 'tp'), may hold values from -12 to 12
- ret_gain: float32 [1024], P('tp'), may hold values from 0.1 to 1.9
- sink_logits: float32 [16], P('tp'), may hold values from 1 to 5
- ret_out: bfloat16 [1024, 2048], P('tp', 'fs'), may hold values from -0.1875 to 0.1875
- att_out: bfloat16 [1024, 2048], P('tp', 'fs'), may hold values from -1.5 to 1.5
Outputs:
- mixed: bfloat16 [4, 16384, 2048], P('fs', 'sp', 'tp')
All inputs are finite; a program needn't handle non-finite values.
Results may differ from a plain program's by a relative error of at most 0.015.
Values may be sent and summed in bfloat16 or wider, within the bound.
A program may use at most 128 MiB of HBM per device.

v0:
```python
import jax
import jax.numpy as jnp
from jax import lax
from jax.sharding import Mesh
from jax.sharding import PartitionSpec as P

DK = 256
DV = 256
HD = 64
WINDOW = 128
BLOCK = 128
SP = ("sp_0", "sp_1")


epsilon = 1e-06


def in_order(tiles, dim):
    lengths = list(tiles.shape[1:])
    lengths[dim] *= tiles.shape[0]
    return jnp.moveaxis(tiles, 0, dim).reshape(lengths)


def from_everyone(array, axis):
    peers = lax.axis_size(axis)
    return lax.all_to_all(
        jnp.broadcast_to(array[None], (peers, *array.shape)), axis, 0, 0, tiled=True
    )


def collect(array, axis, dim):
    return in_order(from_everyone(array, axis), dim)


def neutral_like(array, identity):
    return jax.tree.map(
        lambda a, e: jnp.broadcast_to(jnp.asarray(e, a.dtype), a.shape), array, identity
    )


def entering(array, axes, combine, identity):
    before = start = neutral_like(array, identity)
    subtotal = array
    for axis in reversed(axes):
        peers, mine = (lax.axis_size(axis), lax.axis_index(axis))
        pieces = jax.tree.map(
            lambda part, kind: lax.all_gather(part.astype(kind), axis),
            subtotal,
            (jnp.bfloat16, jnp.bfloat16),
        )
        inside, subtotal = (start, start)
        for k in range(peers):
            passed = k < mine
            subtotal = combine(
                subtotal, jax.tree.map(lambda part, own: part[k].astype(own.dtype), pieces, array)
            )
            inside = jax.tree.map(lambda new, old: jnp.where(passed, new, old), subtotal, inside)
        before = combine(inside, before)
    return before


def passed_along(block, axis, distance):
    devices = range(lax.axis_size(axis))
    route = [(i - distance, i) for i in devices if i - distance in devices]
    return lax.ppermute(block, axis, route)


def in_one_piece(arrays, axis, dim, along):
    both = jnp.concatenate(arrays, axis=along)
    filled, at, done = (lax.all_gather(both, axis, axis=dim, tiled=True), 0, [])
    for a in arrays:
        done.append(lax.slice_in_dim(filled, at, at + a.shape[along], axis=along))
        at += a.shape[along]
    return tuple(done)


def split_up(array, dim, peers):
    before, after = (array.shape[:dim], array.shape[dim + 1 :])
    return jnp.moveaxis(array.reshape(*before, peers, -1, *after), dim, 0)


def sent_and_summed(array, axis, dim):
    tiles = split_up(array, dim, lax.axis_size(axis))
    arrived = lax.all_to_all(tiles, axis, split_axis=0, concat_axis=0, tiled=True)
    return arrived.astype(jnp.float32).sum(axis=0)


def rotate(values, positions):
    half_dim = values.shape[-1] // 2
    inverse = 1.0 / 10000.0 ** (jnp.arange(half_dim, dtype=jnp.float32) / half_dim)
    angles = positions.astype(jnp.float32)[:, None] * inverse[None, :]
    cosine = jnp.cos(angles)[:, None, :]
    sine_table = jnp.sin(angles)[:, None, :]
    front_half = values[..., :half_dim]
    back_half = values[..., half_dim:]
    return jnp.concatenate(
        [
            front_half * cosine - back_half * sine_table,
            front_half * sine_table + back_half * cosine,
        ],
        axis=-1,
    )


def block_step(memory_state, inputs):
    queries, key_matrix_rows, value_matrix_rows, log_rates = inputs
    length_here = log_rates.shape[-1]
    causal = jnp.arange(length_here)[:, None] >= jnp.arange(length_here)[None, :]
    running_totals = jnp.cumsum(log_rates, axis=-1)
    relative = running_totals[:, :, None] - running_totals[:, None, :]
    weight = jnp.where(causal[None], jnp.exp(jnp.where(causal[None], relative, 0.0)), 0.0)
    score_matrix = jnp.einsum("hqd,hkd->hqk", queries, key_matrix_rows) * weight
    carried_state = jnp.einsum(
        "hqd,hdv->hqv", queries * jnp.exp(running_totals)[:, :, None], memory_state
    )
    output_rows = jnp.einsum("arf,afu->aru", score_matrix, value_matrix_rows) + carried_state
    decay_factors = jnp.exp(running_totals[:, -1:] - running_totals)
    memory_state = memory_state * jnp.exp(running_totals[:, -1])[:, None, None] + jnp.einsum(
        "iwj,iwe->ije", key_matrix_rows * decay_factors[:, :, None], value_matrix_rows
    )
    return (memory_state, output_rows)


def chain(earlier, later):
    return (earlier[0] * later[0], earlier[1] * later[0][:, None, None] + later[1])


def shards(
    tokens,
    norm_gain,
    ret_query,
    ret_key,
    ret_value,
    att_query,
    att_key,
    att_value,
    log_decay,
    start_state,
    ret_gain,
    sink_logits,
    ret_out,
    att_out,
):
    gathered = collect(tokens[0], "tp", 1)
    row_count = gathered.shape[0]
    as_float = gathered.astype(jnp.float32)
    normed = (
        as_float
        * lax.rsqrt(jnp.mean(as_float * as_float, axis=-1, keepdims=True) + epsilon)
        * norm_gain
    ).astype(jnp.bfloat16)
    offset = lax.axis_index(SP) * row_count
    positions = offset + jnp.arange(row_count, dtype=jnp.int32)
    weights = (ret_query, ret_key, ret_value, att_query, att_key, att_value)
    pieces = in_one_piece(
        (weights[0], weights[1], weights[2], weights[3], weights[4], weights[5]), SP, 0, 1
    )
    projected = tuple(
        (jnp.dot(normed, piece, preferred_element_type=jnp.float32) for piece in pieces)
    )
    rounded = tuple((product_f.astype(jnp.bfloat16) for product_f in projected))
    projected = rounded[:3]
    head_count = projected[0].shape[1] // DK
    queries = rotate(projected[0].astype(jnp.float32).reshape(row_count, head_count, DK), positions)
    keys_rot = rotate(
        projected[1].astype(jnp.float32).reshape(row_count, head_count, DK), positions
    ) * DK ** (-0.5)
    values_f = projected[2].astype(jnp.float32).reshape(row_count, head_count, DV)
    log_rates = log_decay[0]
    count = row_count // BLOCK

    def blocked(array):
        return array.reshape(count, BLOCK, head_count, array.shape[-1]).transpose(0, 2, 1, 3)

    rates_blocked = log_rates.reshape(head_count, count, BLOCK).transpose(1, 0, 2)
    local_state, pieces = lax.scan(
        block_step,
        jnp.zeros((head_count, DK, DV), jnp.float32),
        (blocked(queries), blocked(keys_rot), blocked(values_f), rates_blocked),
    )
    local_out = pieces.transpose(0, 2, 1, 3).reshape(row_count, head_count, DV)
    running_totals = jnp.cumsum(log_rates, axis=-1)
    device_decay = jnp.exp(running_totals[:, -1])
    identity = (jnp.ones((head_count,), jnp.float32), jnp.zeros((head_count, DK, DV), jnp.float32))
    prior_decay, prior_state = entering((device_decay, local_state), SP, chain, identity)
    incoming = prior_state + prior_decay[:, None, None] * start_state[0]
    retained = local_out + jnp.einsum(
        "thd,hdv->thv", queries * jnp.exp(running_totals).T[:, :, None], incoming
    )
    centred = retained - jnp.mean(retained, axis=-1, keepdims=True)
    variance = jnp.mean(centred * centred, axis=-1, keepdims=True)
    ret_hidden = (
        (centred * lax.rsqrt(variance + epsilon)).reshape(row_count, head_count * DV) * ret_gain
    ).astype(jnp.bfloat16)
    att_queries, att_keys, att_values = rounded[3:]
    kv_heads = att_keys.shape[1] // HD
    groups = att_queries.shape[1] // HD // kv_heads
    earlier_keys, earlier_values = passed_along(
        (att_keys[row_count - WINDOW :], att_values[row_count - WINDOW :]), SP, 1
    )
    extended_keys = jnp.concatenate([earlier_keys, att_keys], axis=0)
    extended_values = jnp.concatenate([earlier_values, att_values], axis=0)
    windows = row_count // WINDOW

    def banded(array):
        earlier = array[:row_count].reshape(windows, WINDOW, kv_heads, HD)
        current = array[WINDOW:].reshape(windows, WINDOW, kv_heads, HD)
        return jnp.concatenate([earlier, current], axis=1)

    key_band = banded(extended_keys)
    value_band = banded(extended_values)
    grouped_q = att_queries.reshape(windows, WINDOW, kv_heads, groups, HD)
    score_matrix = jnp.einsum(
        "nqhgd,nkhd->nhgqk", grouped_q, key_band, preferred_element_type=jnp.float32
    ) * HD ** (-0.5)
    query_index = WINDOW + jnp.arange(WINDOW)
    key_index = jnp.arange(2 * WINDOW)
    allowed = (key_index[None, :] <= query_index[:, None]) & (
        query_index[:, None] - key_index[None, :] < WINDOW
    )
    key_place = offset - WINDOW + jnp.arange(windows)[:, None] * WINDOW + key_index[None, :]
    visible = (allowed[None] & (key_place >= 0)[:, None, :])[:, None, None]
    expo = jnp.exp(jnp.where(visible, score_matrix, -1e30))
    summed = jnp.sum(expo, axis=-1, keepdims=True) + jnp.exp(sink_logits).reshape(
        1, kv_heads, groups, 1, 1
    )
    probs = (expo / summed).astype(jnp.bfloat16)
    attended = jnp.einsum(
        "nhgqk,nkhd->nqhgd", probs, value_band, preferred_element_type=jnp.float32
    )
    att_hidden = attended.astype(jnp.bfloat16).reshape(row_count, kv_heads * groups * HD)
    ret_width = ret_hidden.shape[1]
    joined = jnp.concatenate([ret_hidden, att_hidden], axis=1)[None]
    piece = collect(joined, "fs", 0)
    product = jnp.einsum(
        "srh,hd->srd", piece[:, :, :ret_width], ret_out, preferred_element_type=jnp.float32
    )
    product = product + jnp.einsum(
        "srh,hd->srd", piece[:, :, ret_width:], att_out, preferred_element_type=jnp.float32
    )
    partial_rows = product.astype(jnp.bfloat16)
    regrouped = lax.all_to_all(partial_rows, "fs", split_axis=0, concat_axis=2, tiled=True)
    mixed = sent_and_summed(regrouped[0].astype(jnp.float32).astype(jnp.bfloat16), "tp", 1)
    return mixed.astype(jnp.bfloat16)[None]


def solution(mesh):
    torus = Mesh(
        mesh.devices.reshape(8, 8, mesh.shape["fs"], mesh.shape["tp"]), ("sp_0", "sp_1", "fs", "tp")
    )
    in_specs = (
        P("fs", SP, "tp"),
        P(),
        P(SP, "tp"),
        P(SP, "tp"),
        P(SP, "tp"),
        P(SP, "tp"),
        P(SP, "tp"),
        P(SP, "tp"),
        P("fs", "tp", SP),
        P("fs", "tp", None, None),
        P("tp"),
        P("tp"),
        P("tp", "fs"),
        P("tp", "fs"),
    )
    out_specs = P("fs", SP, "tp")
    return jax.shard_map(
        shards, mesh=torus, in_specs=in_specs, out_specs=out_specs, check_vma=False
    )
```

profile of v0, /device:TPU:1, one launch (start us, length us, event | category | flops | bytes accessed | tf_op | source)
XLA Modules:
  0.0 286.7 jit_solution(14590419649816802804)
XLA Ops:
  6.5 0.8 constant_dynamic-update-slice_fusion.5
  7.4 0.8 constant_dynamic-update-slice_fusion.4
  8.1 0.8 constant_dynamic-update-slice_fusion.3
  8.9 0.8 constant_dynamic-update-slice_fusion.2
  9.6 0.7 constant_dynamic-update-slice_fusion.1
  10.3 0.7 constant_dynamic-update-slice_fusion
  11.1 0.7 copy-done.5
  11.7 1.2 copy.58
  13.0 1.1 broadcast_in_dim.51
  14.1 10.5 %all-to-all-start = ((bf16[2,256,1024]{1,2,0:T(8,128)(2,1)}), bf16[2,256,1024]{1,2,0:T(8,128)(2,1)S(1)}, u32[]{:S(2)}, u32[]{:S(2)}) async-start(bf16[2,256,1024]{1,2,0:T(8,128)(2,1)} %broadcast_in_dim.51), calls=%async_computation | async-start | bytes 2097152 | tf_op jit(solution)/shard_map/all_to_all | solution.py:26
  24.6 1.7 all-to-all-done
  26.3 0.3 multiply_reduce_fusion
  26.7 0.5 multiply_cosine_fusion
  27.2 1.3 fusion.46
  28.5 92.7 %all-gather.7.cloned.1.call-done = bf16[2048,2304]{1,0:T(8,128)(2,1)} async-done(((bf16[32,2304]{1,0:T(8,128)(2,1)}), bf16[2048,2304]{1,0:T(8,128)(2,1)}) %all-gather.7.cloned.1.call-update) | async-done | bytes 9437200 | tf_op jit(solution)/shard_map/all_gather | solution.py:70
  121.3 2.6 fusion.65
  124.0 3.1 %fusion.68 = f32[256,512]{1,0:T(8,128)} fusion(bf16[256,2048]{0,1:T(8,128)(2,1)S(1)} %copy-done.1, bf16[2048,2304]{1,0:T(8,128)(2,1)} %all-gather.7.cloned.1.call-done), kind=kOutput, calls=%fused_computation.67 | convolution fusion | flops 537133056 | bytes 3670016 | tf_op jit(solution)/shard_map/dot_general | solution.py:159
  127.1 1.4 reshape.546
  128.5 3.1 %fusion.62 = f32[256,512]{1,0:T(8,128)} fusion(bf16[256,2048]{0,1:T(8,128)(2,1)S(1)} %copy-done.1, bf16[2048,2304]{1,0:T(8,128)(2,1)} %all-gather.7.cloned.1.call-done), kind=kOutput, calls=%fused_computation.65 | convolution fusion | flops 537133056 | bytes 3670016 | tf_op jit(solution)/shard_map/dot_general | solution.py:159
  131.6 1.4 reshape.548
  133.0 0.4 fusion.204
  133.6 0.5 copy-done.6
  134.0 4.5 %while.13 = (s32[]{:T(128)}, f32[2,256,256]{2,1,0:T(8,128)S(1)}, f32[2,2,128,256]{3,2,1,0:T(8,128)}, f32[2,2,128]{2,1,0:T(2,128)S(1)}, f32[2,2,128,256]{3,2,0,1:...) while((s32[]{:T(128)}, f32[2,256,256]{2,1,0:T(8,128)S(1)}, ...), condition=%wide.region_3.4_spmd.clone, body=%wide.region_1.3_spmd.clone.sunk | while | flops 101597184 | bytes 3457190 | solution.py:176
  134.0 0.3 reduce_window_sum.31
  134.6 0.3 fusion.229
  135.0 0.9 fusion.230
  135.9 0.4 convolution_add_fusion.3
  136.3 0.3 reduce_window_sum.31
  136.9 0.3 fusion.229
  137.2 0.9 fusion.230
  138.2 0.4 convolution_add_fusion.3
  138.6 0.7 convert_element_type.488
  139.4 0.6 reduce-window.6
  140.6 1.4 dynamic-slice
  142.9 13.6 %all-reduce = bf16[16]{0:T(256)(128)(2,1)S(1)} all-reduce(bf16[16]{0:T(256)(128)(2,1)S(1)} %dynamic-update-slice), channel_id=2, replica_groups=mesh['sp_0'=8,'sp_1'=8,'fs'=4,'tp'=2] {'sp_1'}, use_global_device_ids=true, to_apply=%add | all-reduce | flops 16 | bytes 64
  156.6 11.2 %all-gather.2 = bf16[8,1,2]{2,1,0:T(2,128)(2,1)S(1)} all-gather(bf16[1,1,2]{2,1,0:T(2,128)(2,1)S(1)} %fusion.195), channel_id=1, replica_groups=mesh['sp_0'=8,'sp_1'=8,'fs'=4,'tp'=2] {'sp_0'}, dimensions={0}, use_global_device_ids=true | all-gather | bytes 36 | tf_op jit(solution)/shard_map/all_gather | solution.py:47
  167.8 0.7 add.231
  168.6 8.4 %all-gather.11.cloned.1.call-done = bf16[16,256,256]{2,1,0:T(8,128)(2,1)} async-done(((bf16[2,256,256]{2,1,0:T(8,128)(2,1)}), bf16[16,256,256]{2,1,0:T(8,128)(2,1)}) %all-gather.11.cloned.1.call-update) | async-done | bytes 2097168 | tf_op jit(solution)/shard_map/all_gather | solution.py:47
  177.0 2.7 fusion.135
  179.7 0.5 fusion.197
  180.2 0.6 fusion.185
  180.9 0.6 exponential_bitcast_fusion
  181.5 0.6 fusion.192
  182.3 1.5 convolution_convert_fusion.1
  183.8 0.6 slice.277
  184.6 2.7 collective-permute-start.1
  187.2 1.5 convolution_convert_fusion.2
  188.8 0.6 slice.275
  189.4 3.3 %collective-permute-start = (bf16[128,128]{1,0:T(8,128)(2,1)}, bf16[128,128]{1,0:T(8,128)(2,1)S(1)}, u32[]{:S(2)}, u32[]{:S(2)}) collective-permute-start(bf16[128,128]{1,0:T(8,128)(2,1)} %slice.275), channel_id=1, source_target_pairs={{0,8},{8,16},{16,24},{24,32},{32,40},{40,48},{48,56},{56,64},{64,7... | collective-permute-start | bytes 98312 | tf_op jit(solution)/shard_map/ppermute | solution.py:65
  192.7 2.3 fusion.59
  195.9 0.4 reshape.533
  196.8 0.7 fusion.48
  197.7 0.6 fusion.71
  198.6 24.3 %all-gather.9.cloned.1.call-done = bf16[8,2,256,256]{3,2,1,0:T(8,128)(2,1)} async-done(((bf16[1,2,256,256]{3,2,1,0:T(8,128)(2,1)}), bf16[8,2,256,256]{3,2,1,0:T(8,128)(2,1)}) %all-gather.9.cloned.1.call-update) | async-done | bytes 2097168 | tf_op jit(solution)/shard_map/all_gather | solution.py:47
  223.0 3.8 %fusion.206 = (f32[256,2]{0,1:T(2,128)S(1)}, f32[256,2,256]{0,2,1:T(8,128)S(1)}) fusion(f32[256,2,256]{0,2,1:T(8,128)S(1)} %reshape.533, f32[256,2]{0,1:T(2,128)S(1)} %copy-done.15, f32[256,2,128]{2,0,1:T(8,128)S(1)} %get-tuple-element.102, f32[256,2,128]{2,0,1:T(8,128)S(1)} %get-tuple-element.101, f32[1,2,256,256]{3,2,1,0:T(8,128)S(1)} %copy-done.28, ...), kind=kOutput, calls=%fused_computation.314 | convolution fusion | flops 76283392 | bytes 6295712 | tf_op jit(solution)/shard_map/thd,hdv->thv/dot_general | solution.py:187
  227.7 25.2 %all_to_all.30 = bf16[4,1,256,1024]{3,2,1,0:T(8,128)(2,1)S(1)} all-to-all(bf16[4,1,256,1024]{3,2,1,0:T(8,128)(2,1)S(1)} %broadcast_in_dim.54), channel_id=1, replica_groups=mesh['sp_0'=8,'sp_1'=8,'fs'=4,'tp'=2] {'fs'}, dimensions={0} | all-to-all | bytes 4194304 | tf_op jit(solution)/shard_map/all_to_all | solution.py:26
  252.9 0.7 fusion.73
  253.6 0.3 copy-done.3
  253.9 0.7 add_convert_fusion
  254.6 12.2 %all_to_all.31 = bf16[4,256,512]{2,1,0:T(8,128)(2,1)S(1)} all-to-all(bf16[4,256,512]{2,1,0:T(8,128)(2,1)S(1)} %add_convert_fusion), channel_id=1, replica_groups=mesh['sp_0'=8,'sp_1'=8,'fs'=4,'tp'=2] {'fs'}, dimensions={0} | all-to-all | bytes 2097152 | tf_op jit(solution)/shard_map/all_to_all | solution.py:242
  266.8 0.5 copy.83
  267.3 11.4 %all_to_all.32 = bf16[2,256,1024]{1,2,0:T(8,128)(2,1)S(1)} all-to-all(bf16[2,256,1024]{1,2,0:T(8,128)(2,1)S(1)} %bitcast.376), channel_id=1, replica_groups=mesh['sp_0'=8,'sp_1'=8,'fs'=4,'tp'=2] {'tp'}, dimensions={0} | all-to-all | bytes 2097152 | tf_op jit(solution)/shard_map/all_to_all | solution.py:84
  278.7 0.5 reduce_sum.52
  279.2 1.0 copy.84
  (128 shorter events, 4.9 us)
Async XLA Ops:
  6.5 246.3 %copy-start = (bf16[512,512]{1,0:T(8,128)(2,1)S(1)}, bf16[512,512]{1,0:T(8,128)(2,1)}, u32[]{:S(2)}) copy-start(bf16[512,512]{1,0:T(8,128)(2,1)} %param.28) | copy-start | bytes 1572868
  6.5 114.7 %all-gather.7.cloned.1.call-start = ((), (), s32[]{:S(2)}) async-start(), calls=%async_computation.4 | async-start | bytes 9584640 | tf_op jit(solution)/shard_map/all_gather | solution.py:70
  11.0 0.7 copy-start.5
  14.0 13.1 %copy-start.7 = (f32[2048]{0:T(1024)S(1)}, f32[2048]{0:T(1024)}, u32[]{:S(2)}) copy-start(f32[2048]{0:T(1024)} %param.17) | copy-start | bytes 24580
  14.1 12.3 %all-to-all-start = ((bf16[2,256,1024]{1,2,0:T(8,128)(2,1)}), bf16[2,256,1024]{1,2,0:T(8,128)(2,1)S(1)}, u32[]{:S(2)}, u32[]{:S(2)}) async-start(bf16[2,256,1024]{1,2,0:T(8,128)(2,1)} %broadcast_in_dim.51), calls=%async_computation | async-start | bytes 2097152 | tf_op jit(solution)/shard_map/all_to_all | solution.py:26
  24.6 152.4 %all-gather.11.cloned.1.call-start = ((), (), s32[]{:S(2)}) async-start(), calls=%async_computation.6 | async-start | bytes 2359296 | tf_op jit(solution)/shard_map/all_gather | solution.py:47
  28.5 95.5 %copy-start.1 = (bf16[256,2048]{0,1:T(8,128)(2,1)S(1)}, bf16[256,2048]{0,1:T(8,128)(2,1)}, u32[]{:S(2)}) copy-start(bf16[256,2048]{0,1:T(8,128)(2,1)} %fusion.46) | copy-start | bytes 3145732
  133.3 0.7 copy-start.6
  134.0 33.8 %copy-start.29 = (f32[8]{0:T(128)S(1)}, f32[8]{0:T(128)}, u32[]{:S(2)}) copy-start(f32[8]{0:T(128)} %param.27) | copy-start | bytes 100
  138.6 43.7 %copy-start.2 = (bf16[256,2048]{0,1:T(8,128)(2,1)S(1)}, bf16[256,2048]{0,1:T(8,128)(2,1)}, u32[]{:S(2)}) copy-start(bf16[256,2048]{0,1:T(8,128)(2,1)} %fusion.46) | copy-start | bytes 3145732
  139.3 83.6 %all-gather.9.cloned.1.call-start = ((), (), s32[]{:S(2)}) async-start(), calls=%async_computation.5 | async-start | bytes 2359296 | tf_op jit(solution)/shard_map/all_gather | solution.py:47
  168.5 15.3 %copy-start.17 = (f32[2]{0:T(128)}, f32[2]{0:T(128)S(1)}, u32[]{:S(2)}) copy-start(f32[2]{0:T(128)S(1)} %convert_multiply_fusion) | copy-start | bytes 28
  168.6 15.2 %copy-start.9 = (f32[2]{0:T(128)}, f32[2]{0:T(128)S(1)}, u32[]{:S(2)}) copy-start(f32[2]{0:T(128)S(1)} %get-tuple-element.124) | copy-start | bytes 28
  168.6 15.2 %copy-start.11 = (f32[2]{0:T(128)}, f32[2]{0:T(128)S(1)}, u32[]{:S(2)}) copy-start(f32[2]{0:T(128)S(1)} %get-tuple-element.125) | copy-start | bytes 28
  168.6 15.3 %copy-start.13 = (f32[2]{0:T(128)}, f32[2]{0:T(128)S(1)}, u32[]{:S(2)}) copy-start(f32[2]{0:T(128)S(1)} %get-tuple-element.126) | copy-start | bytes 28
  184.6 12.0 %collective-permute-start.1 = (bf16[128,128]{1,0:T(8,128)(2,1)}, bf16[128,128]{1,0:T(8,128)(2,1)S(1)}, u32[]{:S(2)}, u32[]{:S(2)}) collective-permute-start(bf16[128,128]{1,0:T(8,128)(2,1)} %slice.277), channel_id=1, source_target_pairs={{0,8},{8,16},{16,24},{24,32},{32,40},{40,48},{48,56},{56,64},{64,7... | collective-permute-start | bytes 98312 | tf_op jit(solution)/shard_map/ppermute | solution.py:65
  189.4 6.3 %copy-start.4 = (f32[2,2,128,256]{3,2,1,0:T(8,128)S(1)}, f32[2,2,128,256]{3,2,1,0:T(8,128)}, u32[]{:S(2)}) copy-start(f32[2,2,128,256]{3,2,1,0:T(8,128)} %get-tuple-element.43) | copy-start | bytes 1572868
  189.4 6.9 %collective-permute-start = (bf16[128,128]{1,0:T(8,128)(2,1)}, bf16[128,128]{1,0:T(8,128)(2,1)S(1)}, u32[]{:S(2)}, u32[]{:S(2)}) collective-permute-start(bf16[128,128]{1,0:T(8,128)(2,1)} %slice.275), channel_id=1, source_target_pairs={{0,8},{8,16},{16,24},{24,32},{32,40},{40,48},{48,56},{56,64},{64,7... | collective-permute-start | bytes 98312 | tf_op jit(solution)/shard_map/ppermute | solution.py:65
  196.3 1.1 copy-start.16
  197.5 25.4 %copy-start.10 = (f32[2]{0:T(128)S(1)}, f32[2]{0:T(128)}, u32[]{:S(2)}) copy-start(f32[2]{0:T(128)} %copy-done.9) | copy-start | bytes 28
  197.5 25.4 %copy-start.12 = (f32[2]{0:T(128)S(1)}, f32[2]{0:T(128)}, u32[]{:S(2)}) copy-start(f32[2]{0:T(128)} %copy-done.11) | copy-start | bytes 28
  197.5 25.4 %copy-start.14 = (f32[2]{0:T(128)S(1)}, f32[2]{0:T(128)}, u32[]{:S(2)}) copy-start(f32[2]{0:T(128)} %copy-done.13) | copy-start | bytes 28
  197.5 25.4 %copy-start.15 = (f32[256,2]{0,1:T(2,128)S(1)}, f32[256,2]{0,1:T(2,128)}, u32[]{:S(2)}) copy-start(f32[256,2]{0,1:T(2,128)} %exponential_bitcast_fusion) | copy-start | bytes 6148
  197.5 25.4 %copy-start.18 = (f32[2]{0:T(128)S(1)}, f32[2]{0:T(128)}, u32[]{:S(2)}) copy-start(f32[2]{0:T(128)} %copy-done.17) | copy-start | bytes 28
  197.6 25.4 %copy-start.19 = (f32[2]{0:T(128)S(1)}, f32[2]{0:T(128)}, u32[]{:S(2)}) copy-start(f32[2]{0:T(128)} %get-tuple-element.111) | copy-start | bytes 28
  197.6 25.4 %copy-start.20 = (f32[2]{0:T(128)S(1)}, f32[2]{0:T(128)}, u32[]{:S(2)}) copy-start(f32[2]{0:T(128)} %get-tuple-element.112) | copy-start | bytes 28
  197.6 25.4 %copy-start.21 = (f32[2]{0:T(128)S(1)}, f32[2]{0:T(128)}, u32[]{:S(2)}) copy-start(f32[2]{0:T(128)} %get-tuple-element.113) | copy-start | bytes 28
  197.6 25.4 %copy-start.22 = (f32[2]{0:T(128)S(1)}, f32[2]{0:T(128)}, u32[]{:S(2)}) copy-start(f32[2]{0:T(128)} %get-tuple-element.114) | copy-start | bytes 28
  197.6 25.4 %copy-start.23 = (f32[2]{0:T(128)S(1)}, f32[2]{0:T(128)}, u32[]{:S(2)}) copy-start(f32[2]{0:T(128)} %get-tuple-element.115) | copy-start | bytes 28
  197.6 25.4 %copy-start.24 = (f32[2]{0:T(128)S(1)}, f32[2]{0:T(128)}, u32[]{:S(2)}) copy-start(f32[2]{0:T(128)} %get-tuple-element.116) | copy-start | bytes 28
  197.6 25.4 %copy-start.25 = (f32[2]{0:T(128)S(1)}, f32[2]{0:T(128)}, u32[]{:S(2)}) copy-start(f32[2]{0:T(128)} %get-tuple-element.117) | copy-start | bytes 28
  197.6 25.4 %copy-start.26 = (f32[2]{0:T(128)S(1)}, f32[2]{0:T(128)}, u32[]{:S(2)}) copy-start(f32[2]{0:T(128)} %get-tuple-element.97) | copy-start | bytes 28
  197.6 25.4 %copy-start.27 = (f32[2]{0:T(128)S(1)}, f32[2]{0:T(128)}, u32[]{:S(2)}) copy-start(f32[2]{0:T(128)} %get-tuple-element.98) | copy-start | bytes 28
  197.6 25.4 %copy-start.28 = (f32[1,2,256,256]{3,2,1,0:T(8,128)S(1)}, f32[1,2,256,256]{3,2,1,0:T(8,128)}, u32[]{:S(2)}) copy-start(f32[1,2,256,256]{3,2,1,0:T(8,128)} %param.25) | copy-start | bytes 1572868
  197.7 25.4 %copy-start.30 = (f32[2]{0:T(128)S(1)}, f32[2]{0:T(128)}, u32[]{:S(2)}) copy-start(f32[2]{0:T(128)} %fusion.197) | copy-start | bytes 28
  223.0 4.0 %copy-start.8 = (f32[512]{0:T(512)S(1)}, f32[512]{0:T(512)}, u32[]{:S(2)}) copy-start(f32[512]{0:T(512)} %param.26) | copy-start | bytes 6148
  252.9 1.0 copy-start.3
Sparse Core Ops, SparseCore 0:
  11.9 109.3 all-gather.6
  139.4 37.4 all-gather.10
  179.8 43.0 all-gather.8
where the time goes:
time: 288 us; the launch traced here: 287 us
  waiting for transfers between devices  127 us (44%)
  blocking collectives  73.5 us (26%)
  matrix products  24 us (8%)
  local copies, waits for them, and re-layouts  20.4 us (7%)
  starting transfers between devices  16.6 us (6%)
  between operations  14.5 us (5%)
  other arithmetic  10.6 us (4%)
    all_gather x1, waiting for transfers between devices, in_one_piece(): filled, at, done = (lax.all_gather(both, axis, axis=dim, tiled=True), 0, [])  92.7 us
    all_gather x2, waiting for transfers between devices, entering(): lax.all_gather(part.astype(kind), axis)  32.7 us
    all_to_all x1, blocking collectives, from_everyone(): lax.all_to_all(jnp.broadcast_to(array[None], (peers, *array.shape)), axis...  25.2 us
    dot_general x6, matrix products, shards(): jnp.dot(normed, piece, preferred_element_type=jnp.float32)  14.2 us
    unnamed x1, blocking collectives  13.6 us
    all_to_all x1, blocking collectives, shards(): lax.all_to_all(partial_rows, 'fs', split_axis=0, concat_axis=2, tiled=True)  12.2 us
    all_to_all x1, blocking collectives, sent_and_summed(): lax.all_to_all(tiles, axis, split_axis=0, concat_axis=0, tiled=True)  11.4 us
    all_gather x1, blocking collectives, entering(): lax.all_gather(part.astype(kind), axis)  11.2 us
  transfers between devices with their start and end apart: 6, of which 4 were waited for; matrix products, arithmetic and copies ran while one was open for 7% of the time, Pallas kernels for 0%

commit v1 on v0

--- a/solution.py
+++ b/solution.py
@@ -1,6 +1,8 @@
 import jax
 import jax.numpy as jnp
 from jax import lax
+from jax.experimental import pallas as pl
+from jax.experimental.pallas import tpu as pltpu
 from jax.sharding import Mesh
 from jax.sharding import PartitionSpec as P
 
@@ -32,31 +34,81 @@
     return in_order(from_everyone(array, axis), dim)
 
 
-def neutral_like(array, identity):
-    return jax.tree.map(
-        lambda a, e: jnp.broadcast_to(jnp.asarray(e, a.dtype), a.shape), array, identity
-    )
-
-
-def entering(array, axes, combine, identity):
-    before = start = neutral_like(array, identity)
-    subtotal = array
-    for axis in reversed(axes):
-        peers, mine = (lax.axis_size(axis), lax.axis_index(axis))
-        pieces = jax.tree.map(
-            lambda part, kind: lax.all_gather(part.astype(kind), axis),
-            subtotal,
-            (jnp.bfloat16, jnp.bfloat16),
-        )
-        inside, subtotal = (start, start)
-        for k in range(peers):
-            passed = k < mine
-            subtotal = combine(
-                subtotal, jax.tree.map(lambda part, own: part[k].astype(own.dtype), pieces, array)
-            )
-            inside = jax.tree.map(lambda new, old: jnp.where(passed, new, old), subtotal, inside)
-        before = combine(inside, before)
-    return before
+def place(index):
+    return {"sp_0": index // 8, "sp_1": index % 8}
+
+
+def prefix_kernel(own_ref, decay_ref, out_ref, came, rates, back, sems):
+    me = lax.axis_index("sp_0") * 8 + lax.axis_index("sp_1")
+
+    def spread(k, _):
+        to = (me + k) % 64
+        pltpu.make_async_remote_copy(
+            src_ref=decay_ref.at[to // 32],
+            dst_ref=rates.at[me],
+            send_sem=sems.at[0],
+            recv_sem=sems.at[1],
+            device_id=place(to),
+        ).start()
+        pltpu.make_async_remote_copy(
+            src_ref=own_ref.at[to],
+            dst_ref=came.at[me],
+            send_sem=sems.at[2],
+            recv_sem=sems.at[3],
+            device_id=place(to),
+        ).start()
+        return 0
+
+    lax.fori_loop(1, 64, spread, 0)
+    came[me] = own_ref[me]
+    rates[me] = decay_ref[me // 32]
+    few = pl.ds(0, 63)
+    for ref, at in ((rates, 0), (rates, 1), (came, 2), (came, 3)):
+        pltpu.make_async_copy(ref.at[few], ref.at[few], sems.at[at]).wait()
+
+    def advance(k, carried):
+        back[k] = carried.astype(jnp.bfloat16)
+        return carried * rates[k] + came[k].astype(jnp.float32)
+
+    lax.fori_loop(0, 64, advance, jnp.zeros((16, 128), jnp.float32))
+
+    def give_back(k, _):
+        to = (me + k) % 64
+        pltpu.make_async_remote_copy(
+            src_ref=back.at[to],
+            dst_ref=out_ref.at[me],
+            send_sem=sems.at[4],
+            recv_sem=sems.at[5],
+            device_id=place(to),
+        ).start()
+        return 0
+
+    lax.fori_loop(1, 64, give_back, 0)
+    out_ref[me] = back[me]
+    for ref, at in ((back, 4), (out_ref, 5)):
+        pltpu.make_async_copy(ref.at[few], ref.at[few], sems.at[at]).wait()
+
+
+def state_before(decay, state):
+    chunks = state.astype(jnp.bfloat16).reshape(2, 16, 16, 2, 128)
+    chunks = chunks.transpose(0, 1, 3, 2, 4).reshape(64, 16, 128)
+    rates = jnp.broadcast_to(decay[:, None, None], (2, 1, 128))
+    vmem = pl.BlockSpec(memory_space=pltpu.VMEM)
+    prefix = pl.pallas_call(
+        prefix_kernel,
+        out_shape=jax.ShapeDtypeStruct((64, 16, 128), jnp.bfloat16),
+        in_specs=[vmem, vmem],
+        out_specs=vmem,
+        scratch_shapes=[
+            pltpu.VMEM((64, 16, 128), jnp.bfloat16),
+            pltpu.VMEM((64, 1, 128), jnp.float32),
+            pltpu.VMEM((64, 16, 128), jnp.bfloat16),
+            pltpu.SemaphoreType.DMA((6,)),
+        ],
+        compiler_params=pltpu.CompilerParams(has_side_effects=True),
+    )(chunks, rates)
+    prefix = prefix.reshape(2, 16, 2, 16, 128).transpose(0, 1, 3, 2, 4)
+    return prefix.reshape(2, 256, 256).astype(jnp.float32)
 
 
 def passed_along(block, axis, distance):
@@ -119,10 +171,6 @@
         "iwj,iwe->ije", key_matrix_rows * decay_factors[:, :, None], value_matrix_rows
     )
     return (memory_state, output_rows)
-
-
-def chain(earlier, later):
-    return (earlier[0] * later[0], earlier[1] * later[0][:, None, None] + later[1])
 
 
 def shards(
@@ -181,9 +229,11 @@
     local_out = pieces.transpose(0, 2, 1, 3).reshape(row_count, head_count, DV)
     running_totals = jnp.cumsum(log_rates, axis=-1)
     device_decay = jnp.exp(running_totals[:, -1])
-    identity = (jnp.ones((head_count,), jnp.float32), jnp.zeros((head_count, DK, DV), jnp.float32))
-    prior_decay, prior_state = entering((device_decay, local_state), SP, chain, identity)
-    incoming = prior_state + prior_decay[:, None, None] * start_state[0]
+    first = (lax.axis_index(SP) == 0).astype(jnp.float32)
+    opening = start_state[0] * first
+    incoming = opening + state_before(
+        device_decay, local_state + device_decay[:, None, None] * opening
+    )
     retained = local_out + jnp.einsum(
         "thd,hdv->thv", queries * jnp.exp(running_totals).T[:, :, None], incoming
     )

time: 288 us -> 260 us (0.903)
  Pallas kernels: 0 us -> 38.3 us
  waiting for transfers between devices: 127 us -> 93.2 us
  blocking collectives: 73.5 us -> 50.4 us
  matrix products: 24 us -> 19.3 us
  other arithmetic: 10.6 us -> 7.46 us
    pallas_call x0 -> x1, Pallas kernels: none -> 38.3 us  [state_before(): pl.pallas_call(prefix_kernel, out_shape=jax.ShapeDtypeStruct((64, 16, 128...]
    all_gather x2 -> x0, waiting for transfers between devices: 32.7 us -> none  [entering(): lax.all_gather(part.astype(kind), axis)]
    unnamed x1 -> x0, blocking collectives: 13.6 us -> none
    all_gather x1 -> x0, blocking collectives: 11.2 us -> none  [entering(): lax.all_gather(part.astype(kind), axis)]
    dot_general x1, matrix products: 3.84 us -> 0.38 us  [shards(): jnp.einsum('thd,hdv->thv', queries * jnp.exp(running_totals).T[:, :, None...]
    convert_element_type x5 -> x2, other arithmetic: 4.17 us -> 1.12 us  [the longest x1 1 us: state_before(): return prefix.reshape(2, 256, 256).astype(jnp.float32)]
    all_to_all x1, blocking collectives: 11.4 us -> 8.37 us  [sent_and_summed(): lax.all_to_all(tiles, axis, split_axis=0, concat_axis=0, tiled=True)]
    unnamed x73 -> x38, local copies, waits for them, and re-layouts: 7.13 us -> 5.51 us
  transfers between devices with their start and end apart: 6 -> 4, of which waited for: 4 -> 2; matrix products, arithmetic and copies ran while one was open for 7% -> 12% of each run, Pallas kernels for 0% -> 15%
where the time goes in v1:
time: 260 us; the launch traced here: 259 us
  waiting for transfers between devices  93.2 us (36%)
  blocking collectives  50.4 us (19%)
  Pallas kernels  38.3 us (15%)
  matrix products  19.3 us (7%)
  local copies, waits for them, and re-layouts  18.8 us (7%)
  starting transfers between devices  17.4 us (7%)
  between operations  13.9 us (5%)
  other arithmetic  7.46 us (3%)
    all_gather x1, waiting for transfers between devices, in_one_piece(): filled, at, done = (lax.all_gather(both, axis, axis=dim, tiled=True), 0, [])  92.8 us
    pallas_call x1, Pallas kernels, state_before(): pl.pallas_call(prefix_kernel, out_shape=jax.ShapeDtypeStruct((64, 16, 128...  38.3 us
    all_to_all x1, blocking collectives, from_everyone(): lax.all_to_all(jnp.broadcast_to(array[None], (peers, *array.shape)), axis...  27.7 us
    all_to_all x1, blocking collectives, shards(): lax.all_to_all(partial_rows, 'fs', split_axis=0, concat_axis=2, tiled=True)  14.3 us
    dot_general x6, matrix products, shards(): jnp.dot(normed, piece, preferred_element_type=jnp.float32)  13 us
    all_to_all x1, starting transfers between devices, from_everyone(): lax.all_to_all(jnp.broadcast_to(array[None], (peers, *array.shape)), axis...  10.5 us
    all_to_all x1, blocking collectives, sent_and_summed(): lax.all_to_all(tiles, axis, split_axis=0, concat_axis=0, tiled=True)  8.37 us
    ppermute x2, starting transfers between devices, passed_along(): return lax.ppermute(block, axis, route)  6.83 us
  transfers between devices with their start and end apart: 4, of which 2 were waited for; matrix products, arithmetic and copies ran while one was open for 12% of the time, Pallas kernels for 15%

profile of v1, /device:TPU:1, one launch (start us, length us, event | category | flops | bytes accessed | tf_op | source)
XLA Modules:
  0.0 258.9 jit_solution(6385571758910094247)
XLA Ops:
  6.5 0.8 constant_dynamic-update-slice_fusion.5
  7.4 0.8 constant_dynamic-update-slice_fusion.4
  8.1 0.8 constant_dynamic-update-slice_fusion.3
  8.9 0.8 constant_dynamic-update-slice_fusion.2
  9.6 0.7 constant_dynamic-update-slice_fusion.1
  10.3 0.7 constant_dynamic-update-slice_fusion
  11.1 0.7 copy-done.9
  11.7 1.2 copy.62
  13.0 1.0 broadcast_in_dim.56
  14.1 10.5 %all-to-all-start = ((bf16[2,256,1024]{1,2,0:T(8,128)(2,1)}), bf16[2,256,1024]{1,2,0:T(8,128)(2,1)S(1)}, u32[]{:S(2)}, u32[]{:S(2)}) async-start(bf16[2,256,1024]{1,2,0:T(8,128)(2,1)} %broadcast_in_dim.56), calls=%async_computation | async-start | bytes 2097152 | tf_op jit(solution)/shard_map/all_to_all | solution.py:28
  24.7 0.6 reduce-window.6
  25.9 0.4 all-to-all-done
  26.3 0.3 multiply_reduce_fusion
  26.8 0.8 broadcast_and_fusion
  27.5 0.5 multiply_cosine_fusion
  28.1 0.3 fusion.46
  28.4 92.8 %all-gather.2.cloned.1.call-done = bf16[2048,2304]{1,0:T(8,128)(2,1)} async-done(((bf16[32,2304]{1,0:T(8,128)(2,1)}), bf16[2048,2304]{1,0:T(8,128)(2,1)}) %all-gather.2.cloned.1.call-update) | async-done | bytes 9437200 | tf_op jit(solution)/shard_map/all_gather | solution.py:122
  121.3 1.5 convolution_convert_fusion.1
  122.8 0.6 slice.93
  123.5 3.7 %collective-permute-start.1 = (bf16[128,128]{1,0:T(8,128)(2,1)}, bf16[128,128]{1,0:T(8,128)(2,1)}, u32[]{:S(2)}, u32[]{:S(2)}) collective-permute-start(bf16[128,128]{1,0:T(8,128)(2,1)} %slice.93), channel_id=1, source_target_pairs={{0,8},{8,16},{16,24},{24,32},{32,40},{40,48},{48,56},{56,64},{64,7... | collective-permute-start | bytes 98312 | tf_op jit(solution)/shard_map/ppermute | solution.py:117
  127.2 1.5 convolution_convert_fusion.2
  128.8 0.6 slice.91
  129.4 3.1 %collective-permute-start = (bf16[128,128]{1,0:T(8,128)(2,1)}, bf16[128,128]{1,0:T(8,128)(2,1)}, u32[]{:S(2)}, u32[]{:S(2)}) collective-permute-start(bf16[128,128]{1,0:T(8,128)(2,1)} %slice.91), channel_id=1, source_target_pairs={{0,8},{8,16},{16,24},{24,32},{32,40},{40,48},{48,56},{56,64},{64,7... | collective-permute-start | bytes 98312 | tf_op jit(solution)/shard_map/ppermute | solution.py:117
  132.5 2.3 fusion.65
  134.9 2.6 %fusion.68 = f32[256,512]{1,0:T(8,128)S(1)} fusion(bf16[256,2048]{0,1:T(8,128)(2,1)} %copy-done.2, bf16[2048,2304]{1,0:T(8,128)(2,1)} %all-gather.2.cloned.1.call-done), kind=kOutput, calls=%fused_computation.67 | convolution fusion | flops 537133056 | bytes 3670016 | tf_op jit(solution)/shard_map/dot_general | solution.py:207
  137.6 0.3 reshape.304
  137.9 2.6 %fusion.62 = f32[256,512]{1,0:T(8,128)S(1)} fusion(bf16[256,2048]{0,1:T(8,128)(2,1)} %copy-done.2, bf16[2048,2304]{1,0:T(8,128)(2,1)} %all-gather.2.cloned.1.call-done), kind=kOutput, calls=%fused_computation.65 | convolution fusion | flops 537133056 | bytes 3670016 | tf_op jit(solution)/shard_map/dot_general | solution.py:207
  140.6 0.3 reshape.306
  140.9 0.4 fusion.99
  141.5 4.6 %while.13 = (s32[]{:T(128)}, f32[2,256,256]{2,1,0:T(8,128)S(1)}, f32[2,2,128,256]{3,2,1,0:T(8,128)}, f32[2,2,128]{2,1,0:T(2,128)S(1)}, f32[2,2,128,256]{3,2,0,1:...) while((s32[]{:T(128)}, f32[2,256,256]{2,1,0:T(8,128)S(1)}, ...), condition=%wide.region_3.4_spmd.clone, body=%wide.region_1.3_spmd.clone.sunk | while | flops 101597184 | bytes 3457190 | solution.py:224
  141.5 0.3 reduce_window_sum.31
  142.1 0.3 fusion.124
  142.5 0.9 fusion.125
  143.4 0.4 convolution_add_fusion.3
  143.8 0.3 reduce_window_sum.31
  144.4 0.3 fusion.124
  144.7 0.9 fusion.125
  145.7 0.4 convolution_add_fusion.3
  146.1 1.3 copy.70
  147.4 0.4 reshape.289
  148.1 0.7 copy.73
  148.8 0.6 broadcast_in_dim.57.decay_ref
  149.4 38.3 %shard_map.136 = bf16[64,16,128]{2,1,0:T(8,128)(2,1)} custom-call(bf16[64,16,128]{2,1,0:T(8,128)(2,1)} %bitcast.164, f32[2,1,128]{2,1,0:T(1,128)} %broadcast_in_dim.57.decay_ref), custom_call_target="tpu_custom_call" | custom-call | tf_op jit(solution)/shard_map/pallas_call | solution.py:97
  187.7 1.0 convert_bitcast_fusion
  189.0 0.4 reshape.307
  189.5 0.4 fusion.101
  190.3 0.4 copy-done.3
  190.7 2.3 fusion.59
  193.4 0.3 reshape.318
  193.7 0.8 pad_maximum_fusion.3
  194.7 0.8 pad_maximum_fusion.2
  195.7 0.7 fusion.48
  196.4 0.6 fusion.71
  197.0 0.3 copy.87
  197.6 0.3 broadcast_in_dim.60
  197.9 27.7 %all_to_all.30 = bf16[4,1,256,1024]{3,2,1,0:T(8,128)(2,1)S(1)} all-to-all(bf16[4,1,256,1024]{3,2,1,0:T(8,128)(2,1)S(1)} %broadcast_in_dim.60), channel_id=1, replica_groups=mesh['sp_0'=8,'sp_1'=8,'fs'=4,'tp'=2] {'fs'}, dimensions={0} | all-to-all | bytes 4194304 | tf_op jit(solution)/shard_map/all_to_all | solution.py:28
  225.6 0.7 fusion.73
  226.3 0.3 copy-done.4
  226.6 0.7 add_convert_fusion
  227.4 14.3 %all_to_all.31 = bf16[4,256,512]{2,1,0:T(8,128)(2,1)S(1)} all-to-all(bf16[4,256,512]{2,1,0:T(8,128)(2,1)S(1)} %add_convert_fusion), channel_id=1, replica_groups=mesh['sp_0'=8,'sp_1'=8,'fs'=4,'tp'=2] {'fs'}, dimensions={0} | all-to-all | bytes 2097152 | tf_op jit(solution)/shard_map/all_to_all | solution.py:292
  241.7 0.5 copy.89
  242.2 8.4 %all_to_all.32 = bf16[2,256,1024]{1,2,0:T(8,128)(2,1)S(1)} all-to-all(bf16[2,256,1024]{1,2,0:T(8,128)(2,1)S(1)} %bitcast.159), channel_id=1, replica_groups=mesh['sp_0'=8,'sp_1'=8,'fs'=4,'tp'=2] {'tp'}, dimensions={0} | all-to-all | bytes 2097152 | tf_op jit(solution)/shard_map/all_to_all | solution.py:136
  250.6 0.5 reduce_sum.52
  251.1 1.0 copy.90
  (85 shorter events, 3.8 us)
Async XLA Ops:
  6.5 219.1 %copy-start = (bf16[512,512]{1,0:T(8,128)(2,1)S(1)}, bf16[512,512]{1,0:T(8,128)(2,1)}, u32[]{:S(2)}) copy-start(bf16[512,512]{1,0:T(8,128)(2,1)} %param.28) | copy-start | bytes 1572868
  6.5 114.7 %all-gather.2.cloned.1.call-start = ((), (), s32[]{:S(2)}) async-start(), calls=%async_computation.4 | async-start | bytes 9584640 | tf_op jit(solution)/shard_map/all_gather | solution.py:122
  11.0 0.7 copy-start.9
  13.0 11.6 %copy-start.14 = (f32[8]{0:T(128)S(1)}, f32[8]{0:T(128)}, u32[]{:S(2)}) copy-start(f32[8]{0:T(128)} %param.27) | copy-start | bytes 100
  13.0 11.7 %copy-start.11 = (f32[1,2,256]{2,1,0:T(2,128)S(1)}, f32[1,2,256]{2,1,0:T(2,128)}, u32[]{:S(2)}) copy-start(f32[1,2,256]{2,1,0:T(2,128)} %param.24) | copy-start | bytes 6148
  14.1 14.0 %copy-start.12 = (f32[2048]{0:T(1024)S(1)}, f32[2048]{0:T(1024)}, u32[]{:S(2)}) copy-start(f32[2048]{0:T(1024)} %param.17) | copy-start | bytes 24580
  14.1 12.3 %all-to-all-start = ((bf16[2,256,1024]{1,2,0:T(8,128)(2,1)}), bf16[2,256,1024]{1,2,0:T(8,128)(2,1)S(1)}, u32[]{:S(2)}, u32[]{:S(2)}) async-start(bf16[2,256,1024]{1,2,0:T(8,128)(2,1)} %broadcast_in_dim.56), calls=%async_computation | async-start | bytes 2097152 | tf_op jit(solution)/shard_map/all_to_all | solution.py:28
  28.4 106.4 %copy-start.2 = (bf16[256,2048]{0,1:T(8,128)(2,1)}, bf16[256,2048]{0,1:T(8,128)(2,1)S(1)}, u32[]{:S(2)}) copy-start(bf16[256,2048]{0,1:T(8,128)(2,1)S(1)} %fusion.46) | copy-start | bytes 3145732
  122.8 9.7 %copy-start.5 = (bf16[256,128]{1,0:T(8,128)(2,1)}, bf16[256,128]{1,0:T(8,128)(2,1)S(1)}, u32[]{:S(2)}) copy-start(bf16[256,128]{1,0:T(8,128)(2,1)S(1)} %convolution_convert_fusion.1) | copy-start | bytes 196612
  123.5 71.2 %collective-permute-start.1 = (bf16[128,128]{1,0:T(8,128)(2,1)}, bf16[128,128]{1,0:T(8,128)(2,1)}, u32[]{:S(2)}, u32[]{:S(2)}) collective-permute-start(bf16[128,128]{1,0:T(8,128)(2,1)} %slice.93), channel_id=1, source_target_pairs={{0,8},{8,16},{16,24},{24,32},{32,40},{40,48},{48,56},{56,64},{64,7... | collective-permute-start | bytes 98312 | tf_op jit(solution)/shard_map/ppermute | solution.py:117
  128.7 3.8 %copy-start.7 = (bf16[256,128]{1,0:T(8,128)(2,1)}, bf16[256,128]{1,0:T(8,128)(2,1)S(1)}, u32[]{:S(2)}) copy-start(bf16[256,128]{1,0:T(8,128)(2,1)S(1)} %convolution_convert_fusion.2) | copy-start | bytes 196612
  129.4 64.3 %collective-permute-start = (bf16[128,128]{1,0:T(8,128)(2,1)}, bf16[128,128]{1,0:T(8,128)(2,1)}, u32[]{:S(2)}, u32[]{:S(2)}) collective-permute-start(bf16[128,128]{1,0:T(8,128)(2,1)} %slice.91), channel_id=1, source_target_pairs={{0,8},{8,16},{16,24},{24,32},{32,40},{40,48},{48,56},{56,64},{64,7... | collective-permute-start | bytes 98312 | tf_op jit(solution)/shard_map/ppermute | solution.py:117
  146.1 1.8 copy-start.1
  189.5 0.7 copy-start.13
  189.5 1.2 copy-start.3
  190.7 2.4 copy-start.8
  190.7 4.0 %copy-start.6 = (bf16[256,128]{1,0:T(8,128)(2,1)S(1)}, bf16[256,128]{1,0:T(8,128)(2,1)}, u32[]{:S(2)}) copy-start(bf16[256,128]{1,0:T(8,128)(2,1)} %copy-done.5) | copy-start | bytes 196612
  193.1 2.6 %copy-start.10 = (pred[2,128,256]{1,2,0:T(8,128)(4,1)S(1)}, pred[2,128,256]{1,2,0:T(8,128)(4,1)}, u32[]{:S(2)}) copy-start(pred[2,128,256]{1,2,0:T(8,128)(4,1)} %broadcast_and_fusion) | copy-start | bytes 196612
  225.6 1.0 copy-start.4
Sparse Core Ops, SparseCore 0:
  11.9 109.3 all-gather.1

commit v2 on v0

v2 whole, which is shorter than its diff:
```python
import jax
import jax.numpy as jnp
from jax import lax
from jax.experimental import pallas as pl
from jax.experimental.pallas import tpu as pltpu
from jax.sharding import Mesh
from jax.sharding import PartitionSpec as P

D = 2048
DK = 256
HD = 64
ROWS = 256
WINDOW = 128
COLS = 1152
CHUNKS = 4
SP = ("z", "y")
BF = jnp.bfloat16
F32 = jnp.float32
EPS = 1e-06
STEPS = (0, 7, 1, 6, 2, 5, 3, 4)


def dot(a, b, dims=(((1,), (0,)), ((), ())), precision=None):
    return lax.dot_general(a, b, dims, precision=precision, preferred_element_type=F32)


def layer_kernel(
    tok_ref,
    rk_ref,
    rv_ref,
    rq_ref,
    aq_ref,
    kv_ref,
    pack_ref,
    start_ref,
    ro_ref,
    ao_ref,
    gain_ref,
    inverse_ref,
    out_ref,
    tok,
    x_in,
    normed,
    w_all,
    pack,
    start,
    w_out,
    cosine,
    sine,
    keys,
    values,
    queries,
    att_q,
    att_kv,
    state,
    scores,
    pieces,
    came,
    rates,
    own_rate,
    back,
    prior,
    hidden,
    heads,
    s_local,
    s_tok,
    r_tok,
    s_small,
    r_pack,
    r_start,
    s_w,
    r_own,
    r_near,
    r_far,
    s_mirror,
    r_mirror,
    s_scan,
    r_scan,
    s_halo,
    r_halo,
    s_hid,
    r_hid,
    s_out,
    r_out,
):
    z, y = lax.axis_index("z"), lax.axis_index("y")
    x, c = lax.axis_index("x"), lax.axis_index("c")
    me = z * 8 + y
    home = x // 2
    at_home = c == home
    near = 1 - x % 2

    def send(src, dst, send_sem, recv_sem, **to):
        pltpu.make_async_remote_copy(
            src_ref=src, dst_ref=dst, send_sem=send_sem, recv_sem=recv_sem, device_id=to
        ).start()

    def arrived(ref, sem):
        pltpu.make_async_copy(ref, ref, sem).wait()

    def along_first(k):
        return {"z": (z + c * k) % 8, "y": (y + (1 - c) * k) % 8}

    def along_second(k):
        return {"z": (z + (1 - c) * k) % 8, "y": (y + c * k) % 8}

    load_tok = pltpu.make_async_copy(tok_ref, tok, s_local.at[0])
    load_tok.start()
    own = w_all.at[me]
    sources = (rk_ref, rv_ref, rq_ref, aq_ref)
    loads = []
    for n, ref in enumerate(sources):
        cut = pl.ds(pl.multiple_of((x % 2) * 256, 256), 256)
        for half in range(2):
            loads.append(
                pltpu.make_async_copy(
                    ref.at[pl.ds(16 * half, 16), cut],
                    own.at[half, :, pl.ds(256 * n, 256)],
                    s_local.at[1 + 2 * n + half],
                )
            )
    for half in range(2):
        loads.append(
            pltpu.make_async_copy(
                kv_ref.at[x % 2, pl.ds(16 * half, 16)],
                own.at[half, :, pl.ds(1024, 128)],
                s_local.at[9 + half],
            )
        )

    @pl.when(at_home)
    def _():
        for load in loads:
            load.start()

    barrier = pltpu.get_barrier_semaphore()
    friends = [{"x": (x + d) % 4, "c": h} for d in (1, 2, 3) for h in (0, 1)]
    friends += [{"c": 1 - c}]
    friends += [along_first(k) for k in range(1, 8)] + [along_second(k) for k in (1, 7)]
    for friend in friends:
        pl.semaphore_signal(barrier, inc=1, device_id=friend)
    pl.semaphore_wait(barrier, len(friends))

    @pl.when(at_home)
    def _():
        for load in loads:
            load.wait()
        send(own, own, s_small.at[0], r_own, c=1 - c)

    load_tok.wait()
    part = ROWS // CHUNKS

    def token_rows(slot, half, q):
        return x_in.at[slot, half, pl.ds(part * q, part)]

    for q in range(CHUNKS):
        for d in (1, 3):
            send(
                tok.at[pl.ds(part * q, part)],
                token_rows(x % 2, c, q),
                s_tok.at[0],
                r_tok.at[x % 2, c, q],
                x=(x + d) % 4,
                c=home,
            )

    @pl.when(at_home)
    def _():
        for q in range(CHUNKS):
            pltpu.make_async_copy(
                tok.at[pl.ds(part * q, part)], token_rows(x % 2, c, q), r_tok.at[x % 2, c, q]
            ).start()

    @pl.when(jnp.logical_not(at_home))
    def _():
        for q in range(CHUNKS):
            send(
                tok.at[pl.ds(part * q, part)],
                token_rows(x % 2, c, q),
                s_tok.at[1],
                r_tok.at[x % 2, c, q],
                c=1 - c,
            )

    for i in range(2):
        mine = jnp.logical_and(at_home, x % 2 == i)

        @pl.when(mine)
        def _(i=i):
            pltpu.make_async_copy(pack_ref.at[i], pack.at[i], r_pack.at[i]).start()

        @pl.when(jnp.logical_not(mine))
        def _(i=i):
            send(
                pack_ref.at[i],
                pack.at[x % 2],
                s_small.at[1 + i],
                r_pack.at[x % 2],
                x=2 * c + i,
                c=home,
            )

        @pl.when(jnp.logical_and(me == 0, mine))
        def _(i=i):
            pltpu.make_async_copy(start_ref.at[i], start.at[i], r_start.at[i]).start()

        @pl.when(jnp.logical_and(me == 0, jnp.logical_not(mine)))
        def _(i=i):
            send(
                start_ref.at[i],
                start.at[x % 2],
                s_small.at[3 + i],
                r_start.at[x % 2],
                x=2 * c + i,
                c=home,
            )

    def block(ka, kb):
        zz = (z + c * ka + (1 - c) * kb) % 8
        yy = (y + (1 - c) * ka + c * kb) % 8
        return w_all.at[zz * 8 + yy, c]

    def mirror(ref):
        send(ref, ref, s_mirror, r_mirror, c=1 - c)

    @pl.when(jnp.logical_not(at_home))
    def _():
        arrived(own, r_own)

    for k in (1, 7, 2, 6, 3, 5, 4):
        send(block(0, 0), block(0, 0), s_w, r_near.at[8 - k], **along_first(k))

    def limits(n):
        return (4, 3) if n % 2 == 0 else (3, 4)

    def forward(ref, direction, kb, n):
        send(ref, ref, s_w, r_far.at[direction, kb, n], **along_second(7 if direction else 1))

    forward(block(0, 0), 0, 1, 0)
    forward(block(0, 0), 1, 1, 0)

    position = lax.broadcasted_iota(jnp.int32, (ROWS, 128), 0) + me * ROWS
    angle = position.astype(F32) * inverse_ref[...]
    cosine[...] = jnp.cos(angle)
    sine[...] = jnp.sin(angle)

    for n in range(1, 8):
        ka = STEPS[n]
        ref = block(ka, 0)
        arrived(ref, r_near.at[ka])
        forward(ref, 0, 1, n)
        forward(ref, 1, 1, n)
        mirror(ref)

    onward = at_home == (x % 2 == 0)
    relay_half = jnp.where(onward, 1, 0)
    relay_to = (x + jnp.where(onward, 3, 1)) % 4

    def relay(q):
        ref = token_rows(near, relay_half, q)
        arrived(ref, r_tok.at[near, relay_half, q])
        send(ref, ref, s_tok.at[2], r_tok.at[near, relay_half, q], x=relay_to)

    for kb in range(1, 5):
        for n in range(8):
            for direction in range(2):
                limit = limits(n)[direction]
                if kb > limit:
                    continue
                ref = block(STEPS[n], kb if direction else 8 - kb)
                arrived(ref, r_far.at[direction, kb, n])
                if kb < limit:
                    forward(ref, direction, kb + 1, n)
                mirror(ref)
        relay(kb - 1)

    for n, ref in enumerate((ro_ref, ao_ref)):
        rows = pl.ds(pl.multiple_of(c * 512, 512), 512)
        cols = pl.ds(pl.multiple_of((x % 2) * 512, 512), 512)
        dst = w_out.at[n, rows, cols]
        sem = r_out.at[n, x % 2, c]
        for d in (1, 2, 3):
            send(ref, dst, s_out, sem, x=(x + d) % 4, c=home)

        @pl.when(at_home)
        def _(ref=ref, dst=dst, sem=sem):
            pltpu.make_async_copy(ref, dst, sem).start()

        @pl.when(jnp.logical_not(at_home))
        def _(ref=ref, dst=dst, sem=sem):
            send(ref, dst, s_small.at[5], sem, c=1 - c)

    for slot in range(2):
        for half in range(2):
            for q in range(CHUNKS):
                relayed = jnp.logical_and(near == slot, relay_half == half)

                @pl.when(jnp.logical_not(relayed))
                def _(slot=slot, half=half, q=q):
                    arrived(token_rows(slot, half, q), r_tok.at[slot, half, q])

    def norm_rows(t, _):
        slot = t // 8
        rows = pl.ds(pl.multiple_of((t % 8) * 32, 32), 32)
        a = x_in[slot, 0, rows].astype(F32)
        b = x_in[slot, 1, rows].astype(F32)
        total = jnp.sum(a * a, axis=-1, keepdims=True) + jnp.sum(b * b, axis=-1, keepdims=True)
        scale = lax.rsqrt(total * (1.0 / D) + EPS)
        to = pl.ds(pl.multiple_of(t * 32, 32), 32)
        normed[to, 0:1024] = (a * scale * gain_ref[:, 0:1024]).astype(BF)
        normed[to, 1024:2048] = (b * scale * gain_ref[:, 1024:2048]).astype(BF)
        return 0

    lax.fori_loop(0, 16, norm_rows, 0)
    few = pl.ds(0, 63)
    arrived(w_all.at[few, 0], r_mirror)

    def project(at, width):
        w = w_all[:, :, :, at : at + width].reshape(D, width)
        return dot(normed[...], w).astype(BF)

    keys[...] = project(0, 256)
    values[...] = project(256, 256)

    arrived(pack.at[0], r_pack.at[0])
    arrived(pack.at[1], r_pack.at[1])
    ti = lax.broadcasted_iota(jnp.int32, (ROWS, ROWS), 0)
    tj = lax.broadcasted_iota(jnp.int32, (ROWS, ROWS), 1)
    lower = (ti >= tj).astype(F32)
    upper = (ti <= tj).astype(F32)
    exact = lax.Precision.HIGHEST

    def sums(slot):
        rows = pack[slot]
        down = dot(lower, rows, (((1,), (1,)), ((), ())), exact)[:, 0:1]
        across = dot(rows, upper, precision=exact)[0:1, :]
        return down, across

    def rotated(ref, slot):
        rows = ref[pl.ds(ROWS * slot, ROWS)].astype(F32)
        front, rear = rows[:, :128], rows[:, 128:]
        return jnp.concatenate(
            [front * cosine[...] - rear * sine[...], front * sine[...] + rear * cosine[...]], axis=1
        )

    for slot in range(2):
        down, across = sums(slot)
        last = down[ROWS - 1 : ROWS, :]
        key_rows = rotated(keys, slot) * DK ** (-0.5)
        v = values[pl.ds(ROWS * slot, ROWS)]
        own_rate[slot] = jnp.broadcast_to(jnp.exp(last), (1, 128))
        state[slot] = dot((key_rows * jnp.exp(last - down)).astype(BF), v, (((0,), (0,)), ((), ())))
        keys[pl.ds(ROWS * slot, ROWS)] = key_rows.astype(BF)

        @pl.when(me == 0)
        def _(slot=slot):
            arrived(start.at[slot], r_start.at[slot])
            state[slot] = state[slot] + own_rate[slot][:, 0:1] * start[slot]

        for i in range(16):
            for half in range(2):
                pieces[slot * 32 + i * 2 + half] = state[
                    slot, 16 * i : 16 * i + 16, 128 * half : 128 * half + 128
                ].astype(BF)

    def place(index):
        return {"z": index // 8, "y": index % 8}

    def spread(k, _):
        to = (me + k) % 64
        send(own_rate.at[to // 32], rates.at[me], s_scan.at[0], r_scan.at[0], **place(to))
        send(pieces.at[to], came.at[me], s_scan.at[1], r_scan.at[1], **place(to))
        return 0

    lax.fori_loop(1, 64, spread, 0)
    came[me] = pieces[me]
    rates[me] = own_rate[me // 32]

    att_kv[:, pl.ds(WINDOW, ROWS)] = project(1024, 128).reshape(2, ROWS, 128)
    tail = att_kv.at[:, pl.ds(ROWS, WINDOW)]
    lead = att_kv.at[:, pl.ds(0, WINDOW)]

    @pl.when(me < 63)
    def _():
        send(tail, lead, s_halo, r_halo, **place(me + 1))

    @pl.when(me == 0)
    def _():
        att_kv[:, pl.ds(0, WINDOW)] = jnp.zeros((2, WINDOW, 128), BF)

    queries[...] = project(512, 256)
    att_q[...] = project(768, 256)

    for slot in range(2):
        down, across = sums(slot)
        q = rotated(queries, slot)
        weight = jnp.where(ti >= tj, jnp.exp(jnp.where(ti >= tj, down - across, 0.0)), 0.0)
        k = keys[pl.ds(ROWS * slot, ROWS)]
        raw = dot(q.astype(BF), k, (((1,), (1,)), ((), ()))) * weight
        scores[slot] = dot(raw.astype(BF), values[pl.ds(ROWS * slot, ROWS)])
        queries[pl.ds(ROWS * slot, ROWS)] = (q * jnp.exp(down)).astype(BF)

    arrived(rates.at[few], r_scan.at[0])
    arrived(came.at[few], r_scan.at[1])

    def advance(k, carried):
        back[k] = carried.astype(BF)
        return carried * rates[k] + came[k].astype(F32)

    lax.fori_loop(0, 64, advance, jnp.zeros((16, 128), F32))

    def give_back(k, _):
        to = (me + k) % 64
        send(back.at[to], prior.at[me], s_scan.at[2], r_scan.at[2], **place(to))
        return 0

    lax.fori_loop(1, 64, give_back, 0)
    prior[me] = back[me]

    @pl.when(me > 0)
    def _():
        arrived(lead, r_halo)

    qi = lax.broadcasted_iota(jnp.int32, (WINDOW, 2 * WINDOW), 0)
    ki = lax.broadcasted_iota(jnp.int32, (WINDOW, 2 * WINDOW), 1)
    for slot in range(2):
        sink = jnp.exp(pack[slot, 2:3, 0:4])
        for n in range(2):
            allowed = jnp.logical_and(ki > qi, ki <= qi + WINDOW)
            if n == 0:
                allowed = jnp.logical_and(allowed, ki >= jnp.where(me == 0, WINDOW, 0))
            kv = att_kv[slot, pl.ds(WINDOW * n, 2 * WINDOW)]
            rows = att_q[pl.ds(ROWS * slot + WINDOW * n, WINDOW)]
            outs = []
            for g in range(4):
                score = dot(rows[:, HD * g : HD * g + HD], kv[:, :HD], (((1,), (1,)), ((), ())))
                expo = jnp.exp(jnp.where(allowed, score * HD ** (-0.5), -1e30))
                total = jnp.sum(expo, axis=-1, keepdims=True) + sink[:, g : g + 1]
                outs.append(dot((expo / total).astype(BF), kv[:, HD:]))
            hidden[slot, 1, pl.ds(WINDOW * n, WINDOW)] = jnp.concatenate(outs, axis=1).astype(BF)

    def hand_over(kind):
        for i in range(2):
            src = hidden.at[i, kind]
            dst = heads.at[x, kind]
            to = 2 * c + i
            send(src, dst, s_hid.at[kind, i], r_hid.at[kind, x], x=to, c=1 - c)

            @pl.when(to == x)
            def _(src=src, dst=dst):
                pltpu.make_async_copy(src, dst, r_hid.at[kind, x]).start()

            @pl.when(to != x)
            def _(src=src, dst=dst, i=i):
                send(src, dst, s_hid.at[2 + kind, i], r_hid.at[kind, x], x=to)

    hand_over(1)

    arrived(prior.at[few], r_scan.at[2])
    for slot in range(2):
        for i in range(16):
            for half in range(2):
                state[slot, 16 * i : 16 * i + 16, 128 * half : 128 * half + 128] = prior[
                    slot * 32 + i * 2 + half
                ].astype(F32)

        @pl.when(me == 0)
        def _(slot=slot):
            state[slot] = start[slot]

        raw = scores[slot] + dot(queries[pl.ds(ROWS * slot, ROWS)], state[slot].astype(BF))
        centred = raw - jnp.mean(raw, axis=-1, keepdims=True)
        variance = jnp.mean(centred * centred, axis=-1, keepdims=True)
        shaped = centred * lax.rsqrt(variance + EPS) * pack[slot, 1:2, :]
        hidden[slot, 0] = shaped.astype(BF)

    hand_over(0)

    for n in range(2):
        for slot in range(2):
            for half in range(2):
                rows, cols = pl.ds(512 * half, 512), pl.ds(512 * slot, 512)
                arrived(w_out.at[n, rows, cols], r_out.at[n, slot, half])
    total = None
    for kind in (1, 0):
        for j in range(4):
            arrived(heads.at[j, kind], r_hid.at[kind, j])
        rows = jnp.concatenate([heads[j, kind] for j in range(4)], axis=1)
        product = dot(rows, w_out[kind])
        total = product if total is None else total + product
    out_ref[...] = total.astype(BF)

    arrived(x_in.at[0], s_tok.at[0])
    arrived(tok, s_tok.at[2])
    arrived(w_all.at[few, 0], s_w)
    arrived(w_all.at[few, 0], s_mirror)
    arrived(rates.at[few], s_scan.at[0])
    arrived(came.at[few], s_scan.at[1])
    arrived(prior.at[few], s_scan.at[2])

    @pl.when(jnp.logical_not(at_home))
    def _():
        arrived(tok, s_tok.at[1])
        arrived(w_out.at[:, pl.ds(0, 512), pl.ds(0, 512)], s_small.at[5])

    @pl.when(at_home)
    def _():
        arrived(own, s_small.at[0])

    arrived(w_out.at[:, pl.ds(0, 768)], s_out)
    for i in range(2):
        mine = jnp.logical_and(at_home, x % 2 == i)

        @pl.when(jnp.logical_not(mine))
        def _(i=i):
            arrived(pack.at[i], s_small.at[1 + i])

        @pl.when(jnp.logical_and(me == 0, jnp.logical_not(mine)))
        def _(i=i):
            arrived(start.at[i], s_small.at[3 + i])

        for kind in range(2):
            arrived(hidden.at[i, kind], s_hid.at[kind, i])

            @pl.when(2 * c + i != x)
            def _(i=i, kind=kind):
                arrived(hidden.at[i, kind], s_hid.at[2 + kind, i])

    @pl.when(me < 63)
    def _():
        arrived(tail, s_halo)


def shards(
    tokens,
    norm_gain,
    ret_query,
    ret_key,
    ret_value,
    att_query,
    att_key,
    att_value,
    log_decay,
    start_state,
    ret_gain,
    sink_logits,
    ret_out,
    att_out,
):
    kv = jnp.stack(
        [jnp.concatenate([a[:, i : i + HD] for a in (att_key, att_value)], axis=1) for i in (0, HD)]
    )
    pack = jnp.concatenate(
        [
            log_decay[0][:, None, :],
            ret_gain.reshape(2, 1, 256),
            jnp.pad(sink_logits.reshape(2, 1, 4), ((0, 0), (0, 0), (0, 252))),
            jnp.zeros((2, 5, 256), F32),
        ],
        axis=1,
    )
    inverse = (1.0 / 10000.0 ** (jnp.arange(128, dtype=F32) / 128)).reshape(1, 128)
    vmem = pl.BlockSpec(memory_space=pltpu.VMEM)
    hbm = pl.BlockSpec(memory_space=pl.ANY)
    dma = pltpu.SemaphoreType.DMA
    scratch = [
        pltpu.VMEM((ROWS, 1024), BF),
        pltpu.VMEM((2, 2, ROWS, 1024), BF),
        pltpu.VMEM((2 * ROWS, D), BF),
        pltpu.VMEM((64, 2, 16, COLS), BF),
        pltpu.VMEM((2, 8, 256), F32),
        pltpu.VMEM((2, 256, 256), F32),
        pltpu.VMEM((2, 1024, 1024), BF),
        pltpu.VMEM((ROWS, 128), F32),
        pltpu.VMEM((ROWS, 128), F32),
        pltpu.VMEM((2 * ROWS, 256), BF),
        pltpu.VMEM((2 * ROWS, 256), BF),
        pltpu.VMEM((2 * ROWS, 256), BF),
        pltpu.VMEM((2 * ROWS, 256), BF),
        pltpu.VMEM((2, WINDOW + ROWS, 128), BF),
        pltpu.VMEM((2, 256, 256), F32),
        pltpu.VMEM((2, ROWS, 256), F32),
        pltpu.VMEM((64, 16, 128), BF),
        pltpu.VMEM((64, 16, 128), BF),
        pltpu.VMEM((64, 1, 128), F32),
        pltpu.VMEM((2, 1, 128), F32),
        pltpu.VMEM((64, 16, 128), BF),
        pltpu.VMEM((64, 16, 128), BF),
        pltpu.VMEM((2, 2, ROWS, 256), BF),
        pltpu.VMEM((4, 2, ROWS, 256), BF),
        dma((11,)),
        dma((3,)),
        dma((2, 2, CHUNKS)),
        dma((6,)),
        dma((2,)),
        dma((2,)),
        dma,
        dma,
        dma((8,)),
        dma((2, 5, 8)),
        dma,
        dma,
        dma((3,)),
        dma((3,)),
        dma,
        dma,
        dma((4, 2)),
        dma((2, 4)),
        dma,
        dma((2, 2, 2)),
    ]
    mixed = pl.pallas_call(
        layer_kernel,
        out_shape=jax.ShapeDtypeStruct((ROWS, 1024), BF),
        in_specs=[hbm] * 5 + [hbm, hbm, hbm, hbm, hbm, vmem, vmem],
        out_specs=vmem,
        scratch_shapes=scratch,
        compiler_params=pltpu.CompilerParams(
            collective_id=0, has_side_effects=True, vmem_limit_bytes=60 * 1024 * 1024
        ),
    )(
        tokens[0],
        ret_key,
        ret_value,
        ret_query,
        att_query,
        kv,
        pack,
        start_state[0],
        ret_out,
        att_out,
        norm_gain.reshape(1, D),
        inverse,
    )
    return mixed[None]


def solution(mesh):
    torus = Mesh(
        mesh.devices.reshape(8, 8, mesh.shape["fs"], mesh.shape["tp"]), ("z", "y", "x", "c")
    )
    across = P(SP, "c")
    in_specs = (
        P("x", SP, "c"),
        P(),
        across,
        across,
        across,
        across,
        across,
        across,
        P("x", "c", SP),
        P("x", "c", None, None),
        P("c"),
        P("c"),
        P("c", "x"),
        P("c", "x"),
    )
    return jax.shard_map(
        shards, mesh=torus, in_specs=in_specs, out_specs=P("x", SP, "c"), check_vma=False
    )
```

time: 288 us -> 104 us (0.36)
  waiting for transfers between devices: 127 us -> 0 us
  Pallas kernels: 0 us -> 97.4 us
  blocking collectives: 73.5 us -> 0 us
  matrix products: 24 us -> 0 us
  starting transfers between devices: 16.6 us -> 0 us
  local copies, waits for them, and re-layouts: 20.4 us -> 4.18 us
  between operations: 14.5 us -> 0.02 us
  other arithmetic: 10.6 us -> 1.94 us
    all_gather x3 -> x0, waiting for transfers between devices: 125 us -> none  [the longest x1 92.7 us: in_one_piece(): filled, at, done = (lax.all_gather(both, axis, axis=dim, tiled=True), 0, [])]
    pallas_call x0 -> x1, Pallas kernels: none -> 97.4 us  [shards(): pl.pallas_call(layer_kernel, out_shape=jax.ShapeDtypeStruct((ROWS, 1024),...]
    all_to_all x3 -> x0, blocking collectives: 48.7 us -> none  [the longest x1 25.2 us: from_everyone(): lax.all_to_all(jnp.broadcast_to(array[None], (peers, *array.shape)), axis...]
    dot_general x17 -> x0, matrix products: 24 us -> none  [the longest x6 14.2 us: shards(): jnp.dot(normed, piece, preferred_element_type=jnp.float32)]
    unnamed x1 -> x0, blocking collectives: 13.6 us -> none
    all_gather x1 -> x0, blocking collectives: 11.2 us -> none  [entering(): lax.all_gather(part.astype(kind), axis)]
    all_to_all x1 -> x0, starting transfers between devices: 10.5 us -> none  [from_everyone(): lax.all_to_all(jnp.broadcast_to(array[None], (peers, *array.shape)), axis...]
    ppermute x2 -> x0, starting transfers between devices: 6 us -> none  [passed_along(): return lax.ppermute(block, axis, route)]
  transfers between devices with their start and end apart: 6 -> 0, of which waited for: 4 -> 0; matrix products, arithmetic and copies ran while one was open for 7% -> 0% of each run, Pallas kernels for 0% -> 0%
where the time goes in v2:
time: 104 us
  Pallas kernels  97.4 us (94%)
  local copies, waits for them, and re-layouts  4.18 us (4%)
  other arithmetic  1.94 us (2%)
    pallas_call x1, Pallas kernels, shards(): pl.pallas_call(layer_kernel, out_shape=jax.ShapeDtypeStruct((ROWS, 1024),...  97.4 us
    unnamed x11, local copies, waits for them, and re-layouts  3.87 us

profile of v2, /device:TPU:1, one launch (start us, length us, event | category | flops | bytes accessed | tf_op | source)
XLA Modules:
  0.0 103.5 jit_solution(8228940576389699922)
XLA Ops:
  0.0 0.1 pad.8.clone
  0.1 0.0 copy-start.4
  0.1 0.6 negate_power_fusion.inverse_ref
  0.7 0.1 copy-done.4
  0.7 0.0 copy-start.2
  0.7 0.1 reshape.24
  0.8 0.6 copy-done.2
  1.4 0.0 copy-start.3
  1.4 0.7 copy-done.3
  2.1 0.0 copy-start
  2.1 0.7 fusion.pack_ref
  2.8 0.0 copy-done
  2.8 0.0 copy-start.1
  2.8 0.1 fusion.2
  2.9 0.6 copy-done.1
  3.5 0.1 fusion.3
  3.6 0.1 maximum_bitcast_fusion
  3.7 0.6 pad_maximum_fusion.kv_ref
  4.3 97.4 %shard_map.136 = bf16[256,1024]{1,0:T(8,128)(2,1)} custom-call(bf16[256,1024]{1,0:T(8,128)(2,1)} %bitcast.11, bf16[32,512]{1,0:T(8,128)(2,1)} %rk_ref.1, bf16[32,512]{1,0:T(8,128)(2,1)} %rv_ref.1, bf16[32,512]{1,0:T(8,128)(2,1)} %rq_ref.1, bf16[32,512]{1,0:T(8,128)(2,1)} %aq_ref.1, bf16[2,32,128]{2,1,0:T(8,128)(2,1)} %pad_maximum_fusion.kv_ref, ...), custom_call_target="tpu_custom_call" | custom-call | tf_op jit(solution)/shard_map/pallas_call | solution.py:612
  101.7 1.9 %copy.17 = bf16[1,256,1024]{2,1,0:T(8,128)(2,1)} copy(bf16[1,256,1024]{2,1,0:T(8,128)(2,1)} %bitcast.10) | data formatting | bytes 1048576
  (2 shorter events, 0.0 us)
Async XLA Ops:
  0.1 0.7 copy-start.4
  0.7 0.7 copy-start.2
  1.4 0.7 copy-start.3
  2.1 0.7 copy-start
  2.8 0.7 copy-start.1

commit v3 on v2

--- a/solution.py
+++ b/solution.py
@@ -1,5 +1,6 @@
 import jax
 import jax.numpy as jnp
+import numpy as np
 from jax import lax
 from jax.experimental import pallas as pl
 from jax.experimental.pallas import tpu as pltpu
@@ -30,8 +31,11 @@
     rv_ref,
     rq_ref,
     aq_ref,
-    kv_ref,
-    pack_ref,
+    ak_ref,
+    av_ref,
+    decay_ref,
+    ret_gain_ref,
+    sink_ref,
     start_ref,
     ro_ref,
     ao_ref,
@@ -44,7 +48,19 @@
     w_all,
     pack,
     start,
-    w_out,
+    o_near,
+    o_far,
+    kv_raw,
+    decay_raw,
+    ret_gain_raw,
+    sink_raw,
+    pack_own,
+    gain,
+    inverse,
+    inside,
+    grow,
+    fall,
+    partial,
     cosine,
     sine,
     keys,
@@ -82,6 +98,14 @@
     r_hid,
     s_out,
     r_out,
+    r_own_far,
+    s_slice,
+    r_slice,
+    s_o,
+    r_o_near,
+    r_o_far,
+    s_o_mirror,
+    r_o_mirror,
 ):
     z, y = lax.axis_index("z"), lax.axis_index("y")
     x, c = lax.axis_index("x"), lax.axis_index("c")
@@ -104,50 +128,77 @@
     def along_second(k):
         return {"z": (z + (1 - c) * k) % 8, "y": (y + c * k) % 8}
 
-    load_tok = pltpu.make_async_copy(tok_ref, tok, s_local.at[0])
-    load_tok.start()
-    own = w_all.at[me]
-    sources = (rk_ref, rv_ref, rq_ref, aq_ref)
-    loads = []
-    for n, ref in enumerate(sources):
-        cut = pl.ds(pl.multiple_of((x % 2) * 256, 256), 256)
-        for half in range(2):
-            loads.append(
-                pltpu.make_async_copy(
-                    ref.at[pl.ds(16 * half, 16), cut],
-                    own.at[half, :, pl.ds(256 * n, 256)],
-                    s_local.at[1 + 2 * n + half],
-                )
-            )
-    for half in range(2):
-        loads.append(
-            pltpu.make_async_copy(
-                kv_ref.at[x % 2, pl.ds(16 * half, 16)],
-                own.at[half, :, pl.ds(1024, 128)],
-                s_local.at[9 + half],
-            )
-        )
-
-    @pl.when(at_home)
-    def _():
-        for load in loads:
-            load.start()
-
     barrier = pltpu.get_barrier_semaphore()
     friends = [{"x": (x + d) % 4, "c": h} for d in (1, 2, 3) for h in (0, 1)]
     friends += [{"c": 1 - c}]
     friends += [along_first(k) for k in range(1, 8)] + [along_second(k) for k in (1, 7)]
     for friend in friends:
         pl.semaphore_signal(barrier, inc=1, device_id=friend)
-    pl.semaphore_wait(barrier, len(friends))
+
+    own = w_all.at[me]
+    odd = x % 2
+    small = (
+        (ak_ref, kv_raw.at[0]),
+        (av_ref, kv_raw.at[1]),
+        (decay_ref, decay_raw),
+        (ret_gain_ref, ret_gain_raw),
+        (sink_ref, sink_raw),
+        (inverse_ref, inverse),
+        (gain_ref, gain),
+        (tok_ref, tok),
+    )
+    small = [
+        pltpu.make_async_copy(src, dst, s_local.at[8 + n]) for n, (src, dst) in enumerate(small)
+    ]
+    loads = []
+    for n, ref in enumerate((rk_ref, rv_ref, rq_ref, aq_ref)):
+        cols = pl.ds(pl.multiple_of(odd * 256, 256), 256)
+        for half in range(2):
+            loads.append(
+                pltpu.make_async_copy(
+                    ref.at[pl.ds(16 * half, 16), cols],
+                    own.at[half, :, pl.ds(256 * n, 256)],
+                    s_local.at[2 * n + half],
+                )
+            )
+    for load in small[:2]:
+        load.start()
+
+    @pl.when(at_home)
+    def _():
+        for load in loads:
+            load.start()
+
+    for load in small[2:]:
+        load.start()
+    for load in small[:7]:
+        load.wait()
+    position = lax.broadcasted_iota(jnp.int32, (ROWS, 128), 0) + me * ROWS
+    angle = position.astype(F32) * inverse[...]
+    cosine[...] = jnp.cos(angle)
+    sine[...] = jnp.sin(angle)
+    pack_own[...] = jnp.zeros((2, 8, 256), F32)
+    for i in range(2):
+        pack_own[i, 0:1, :] = decay_raw[i : i + 1, :]
+        pack_own[i, 1:2, :] = ret_gain_raw[:, 256 * i : 256 * i + 256]
+        pack_own[i, 2:3, 0:4] = sink_raw[:, 4 * i : 4 * i + 4]
 
     @pl.when(at_home)
     def _():
         for load in loads:
             load.wait()
+        both = [jnp.where(odd == 0, kv_raw[n, :, :HD], kv_raw[n, :, HD:]) for n in range(2)]
+        both = jnp.concatenate(both, axis=1)
+        for half in range(2):
+            w_all[me, half, :, 1024:COLS] = both[16 * half : 16 * half + 16]
+
+    small[7].wait()
+    pl.semaphore_wait(barrier, len(friends))
+
+    @pl.when(at_home)
+    def _():
         send(own, own, s_small.at[0], r_own, c=1 - c)
 
-    load_tok.wait()
     part = ROWS // CHUNKS
 
     def token_rows(slot, half, q):
@@ -187,12 +238,12 @@
 
         @pl.when(mine)
         def _(i=i):
-            pltpu.make_async_copy(pack_ref.at[i], pack.at[i], r_pack.at[i]).start()
+            pltpu.make_async_copy(pack_own.at[i], pack.at[i], r_pack.at[i]).start()
 
         @pl.when(jnp.logical_not(mine))
         def _(i=i):
             send(
-                pack_ref.at[i],
+                pack_own.at[i],
                 pack.at[x % 2],
                 s_small.at[1 + i],
                 r_pack.at[x % 2],
@@ -239,11 +290,6 @@
     forward(block(0, 0), 0, 1, 0)
     forward(block(0, 0), 1, 1, 0)
 
-    position = lax.broadcasted_iota(jnp.int32, (ROWS, 128), 0) + me * ROWS
-    angle = position.astype(F32) * inverse_ref[...]
-    cosine[...] = jnp.cos(angle)
-    sine[...] = jnp.sin(angle)
-
     for n in range(1, 8):
         ka = STEPS[n]
         ref = block(ka, 0)
@@ -261,96 +307,185 @@
         arrived(ref, r_tok.at[near, relay_half, q])
         send(ref, ref, s_tok.at[2], r_tok.at[near, relay_half, q], x=relay_to)
 
-    for kb in range(1, 5):
-        for n in range(8):
-            for direction in range(2):
-                limit = limits(n)[direction]
-                if kb > limit:
-                    continue
-                ref = block(STEPS[n], kb if direction else 8 - kb)
-                arrived(ref, r_far.at[direction, kb, n])
-                if kb < limit:
-                    forward(ref, direction, kb + 1, n)
-                mirror(ref)
-        relay(kb - 1)
-
-    for n, ref in enumerate((ro_ref, ao_ref)):
-        rows = pl.ds(pl.multiple_of(c * 512, 512), 512)
-        cols = pl.ds(pl.multiple_of((x % 2) * 512, 512), 512)
-        dst = w_out.at[n, rows, cols]
-        sem = r_out.at[n, x % 2, c]
-        for d in (1, 2, 3):
-            send(ref, dst, s_out, sem, x=(x + d) % 4, c=home)
-
-        @pl.when(at_home)
-        def _(ref=ref, dst=dst, sem=sem):
-            pltpu.make_async_copy(ref, dst, sem).start()
-
-        @pl.when(jnp.logical_not(at_home))
-        def _(ref=ref, dst=dst, sem=sem):
-            send(ref, dst, s_small.at[5], sem, c=1 - c)
-
-    for slot in range(2):
-        for half in range(2):
-            for q in range(CHUNKS):
-                relayed = jnp.logical_and(near == slot, relay_half == half)
-
-                @pl.when(jnp.logical_not(relayed))
-                def _(slot=slot, half=half, q=q):
-                    arrived(token_rows(slot, half, q), r_tok.at[slot, half, q])
-
-    def norm_rows(t, _):
-        slot = t // 8
-        rows = pl.ds(pl.multiple_of((t % 8) * 32, 32), 32)
+    def norm_rows(slot, t):
+        if t % 2 == 0:
+            q = t // 2
+
+            @pl.when(slot == near)
+            def _():
+                arrived(token_rows(near, 1 - relay_half, q), r_tok.at[near, 1 - relay_half, q])
+
+            @pl.when(slot != near)
+            def _():
+                for half in range(2):
+                    arrived(token_rows(1 - near, half, q), r_tok.at[1 - near, half, q])
+
+        rows = pl.ds(32 * t, 32)
         a = x_in[slot, 0, rows].astype(F32)
         b = x_in[slot, 1, rows].astype(F32)
         total = jnp.sum(a * a, axis=-1, keepdims=True) + jnp.sum(b * b, axis=-1, keepdims=True)
         scale = lax.rsqrt(total * (1.0 / D) + EPS)
-        to = pl.ds(pl.multiple_of(t * 32, 32), 32)
-        normed[to, 0:1024] = (a * scale * gain_ref[:, 0:1024]).astype(BF)
-        normed[to, 1024:2048] = (b * scale * gain_ref[:, 1024:2048]).astype(BF)
-        return 0
-
-    lax.fori_loop(0, 16, norm_rows, 0)
-    few = pl.ds(0, 63)
-    arrived(w_all.at[few, 0], r_mirror)
-
-    def project(at, width):
-        w = w_all[:, :, :, at : at + width].reshape(D, width)
-        return dot(normed[...], w).astype(BF)
-
-    keys[...] = project(0, 256)
-    values[...] = project(256, 256)
+        to = pl.ds(pl.multiple_of(slot * ROWS + 32 * t, 32), 32)
+        normed[to, 0:1024] = (a * scale * gain[:, 0:1024]).astype(BF)
+        normed[to, 1024:2048] = (b * scale * gain[:, 1024:2048]).astype(BF)
+
+    def ring(kb, n):
+        for direction in range(2):
+            limit = limits(n)[direction]
+            if kb > limit:
+                continue
+            ref = block(STEPS[n], kb if direction else 8 - kb)
+            arrived(ref, r_far.at[direction, kb, n])
+            if kb < limit:
+                forward(ref, direction, kb + 1, n)
+            mirror(ref)
+
+    relay(0)
+    for n in range(4):
+        ring(1, n)
+    relay(1)
+    for n in range(4, 8):
+        ring(1, n)
+    relay(2)
 
     arrived(pack.at[0], r_pack.at[0])
     arrived(pack.at[1], r_pack.at[1])
     ti = lax.broadcasted_iota(jnp.int32, (ROWS, ROWS), 0)
     tj = lax.broadcasted_iota(jnp.int32, (ROWS, ROWS), 1)
-    lower = (ti >= tj).astype(F32)
-    upper = (ti <= tj).astype(F32)
     exact = lax.Precision.HIGHEST
 
-    def sums(slot):
+    def decays(slot):
         rows = pack[slot]
+        lower = (ti >= tj).astype(F32)
+        upper = (ti <= tj).astype(F32)
         down = dot(lower, rows, (((1,), (1,)), ((), ())), exact)[:, 0:1]
         across = dot(rows, upper, precision=exact)[0:1, :]
-        return down, across
+        last = down[ROWS - 1 : ROWS, :]
+        inside[slot] = jnp.where(ti >= tj, jnp.exp(jnp.where(ti >= tj, down - across, 0.0)), 0.0)
+        grow[slot] = jnp.broadcast_to(jnp.exp(down), (ROWS, 128))
+        fall[slot] = jnp.broadcast_to(jnp.exp(last - down), (ROWS, 128))
+        own_rate[slot] = jnp.broadcast_to(jnp.exp(last), (1, 128))
+
+    for n in range(8):
+        ring(2, n)
+        if n == 1:
+            decays(0)
+        if n == 3:
+            relay(3)
+        if n == 5:
+            decays(1)
+
+    first_at = c * z + (1 - c) * y
+    second_at = (1 - c) * z + c * y
+    line = second_at * 8 + first_at
+
+    @pl.when(line < 32)
+    def _():
+        for d in (1, 2, 3):
+            src = ro_ref.at[32 + line % 32]
+            send(src, o_far.at[c, line, 3 - d], s_slice, r_slice.at[3 - d], x=(x + d) % 4)
+
+    @pl.when(line >= 32)
+    def _():
+        for d in (1, 2, 3):
+            src = ao_ref.at[32 + line % 32]
+            send(src, o_far.at[c, line, 3 - d], s_slice, r_slice.at[3 - d], x=(x + d) % 4)
+
+    low, high, three = pl.ds(0, 32), pl.ds(32, 32), pl.ds(0, 3)
+    for n, ref in enumerate((ro_ref, ao_ref)):
+        for d in (1, 2, 3):
+            send(
+                ref.at[low],
+                o_near.at[c, n, 3 - d],
+                s_out,
+                r_out.at[c, n, 3 - d],
+                x=(x + d) % 4,
+                c=home,
+            )
+        pairs = (
+            (ref.at[low], o_near.at[c, n, 3], r_out.at[c, n, 3]),
+            (ref.at[high], o_far.at[c, pl.ds(32 * n, 32), 3], r_own_far.at[c, n]),
+        )
+
+        @pl.when(at_home)
+        def _(pairs=pairs):
+            for src, dst, sem in pairs:
+                pltpu.make_async_copy(src, dst, sem).start()
+
+        @pl.when(jnp.logical_not(at_home))
+        def _(pairs=pairs):
+            for src, dst, sem in pairs:
+                send(src, dst, s_small.at[5], sem, c=1 - c)
+
+    def o_block(ka):
+        return o_far.at[c, second_at * 8 + (first_at + ka) % 8, three]
+
+    def o_group(kb, g):
+        at = pl.multiple_of(((second_at + kb) % 8) * 8 + 4 * g, 4)
+        return o_far.at[c, pl.ds(at, 4), three]
+
+    def o_forward(ref, direction, kb, g):
+        send(ref, ref, s_o, r_o_far.at[direction, kb, g], **along_second(7 if direction else 1))
+
+    def o_mirror(ref):
+        send(ref, ref, s_o_mirror, r_o_mirror, c=1 - c)
+
+    def o_step(kb):
+        for g in range(2):
+            for direction in range(2):
+                limit = limits(g)[direction]
+                if kb > limit:
+                    continue
+                ref = o_group(kb if direction else 8 - kb, g)
+                arrived(ref, r_o_far.at[direction, kb, g])
+                if kb < limit:
+                    o_forward(ref, direction, kb + 1, g)
+                o_mirror(ref)
+
+    for n in range(8):
+        ring(3, n)
+        norm_rows(near, n)
+    for d in range(3):
+        arrived(o_far.at[c, line, d], r_slice.at[d])
+    for k in (4, 3, 5, 2, 6, 1, 7):
+        send(o_block(0), o_block(0), s_o, r_o_near.at[8 - k], **along_first(k))
+    for n in range(8):
+        ring(4, n)
+        norm_rows(1 - near, n)
+    for k in range(1, 8):
+        arrived(o_block(k), r_o_near.at[k])
+    for g in range(2):
+        o_forward(o_group(0, g), 0, 1, g)
+        o_forward(o_group(0, g), 1, 1, g)
+        o_mirror(o_group(0, g))
+    few = pl.ds(0, 63)
+    arrived(w_all.at[few, 0], r_mirror)
+
+    def project(at, width):
+        w = w_all[:, :, :, at : at + width].reshape(D, width)
+        return dot(normed[...], w).astype(BF)
+
+    keys[...] = project(0, 256)
+    values[...] = project(256, 256)
 
     def rotated(ref, slot):
         rows = ref[pl.ds(ROWS * slot, ROWS)].astype(F32)
         front, rear = rows[:, :128], rows[:, 128:]
-        return jnp.concatenate(
-            [front * cosine[...] - rear * sine[...], front * sine[...] + rear * cosine[...]], axis=1
+        return (
+            front * cosine[...] - rear * sine[...],
+            front * sine[...] + rear * cosine[...],
         )
 
     for slot in range(2):
-        down, across = sums(slot)
-        last = down[ROWS - 1 : ROWS, :]
-        key_rows = rotated(keys, slot) * DK ** (-0.5)
+        front, rear = [part * DK ** (-0.5) for part in rotated(keys, slot)]
         v = values[pl.ds(ROWS * slot, ROWS)]
-        own_rate[slot] = jnp.broadcast_to(jnp.exp(last), (1, 128))
-        state[slot] = dot((key_rows * jnp.exp(last - down)).astype(BF), v, (((0,), (0,)), ((), ())))
-        keys[pl.ds(ROWS * slot, ROWS)] = key_rows.astype(BF)
+        left = jnp.concatenate(
+            [(front * fall[slot]).astype(BF), (rear * fall[slot]).astype(BF)], axis=1
+        )
+        state[slot] = dot(left, v, (((0,), (0,)), ((), ())))
+        keys[pl.ds(ROWS * slot, ROWS)] = jnp.concatenate(
+            [front.astype(BF), rear.astype(BF)], axis=1
+        )
 
         @pl.when(me == 0)
         def _(slot=slot):
@@ -366,13 +501,21 @@
     def place(index):
         return {"z": index // 8, "y": index % 8}
 
-    def spread(k, _):
-        to = (me + k) % 64
-        send(own_rate.at[to // 32], rates.at[me], s_scan.at[0], r_scan.at[0], **place(to))
-        send(pieces.at[to], came.at[me], s_scan.at[1], r_scan.at[1], **place(to))
-        return 0
-
-    lax.fori_loop(1, 64, spread, 0)
+    def reach(k):
+        return min(k // 8, 8 - k // 8) + min(k % 8, 8 - k % 8)
+
+    offsets = sorted(range(1, 64), key=lambda k: (-reach(k), k))
+
+    def peer(k):
+        zz, yy = (z + k // 8) % 8, (y + k % 8) % 8
+        return zz * 8 + yy, {"z": zz, "y": yy}
+
+    for k in offsets:
+        to, at = peer(k)
+        send(pieces.at[to], came.at[me], s_scan.at[1], r_scan.at[1], **at)
+    for k in offsets:
+        to, at = peer(k)
+        send(own_rate.at[to // 32], rates.at[me], s_scan.at[0], r_scan.at[0], **at)
     came[me] = pieces[me]
     rates[me] = own_rate[me // 32]
 
@@ -388,18 +531,22 @@
     def _():
         att_kv[:, pl.ds(0, WINDOW)] = jnp.zeros((2, WINDOW, 128), BF)
 
-    queries[...] = project(512, 256)
-    att_q[...] = project(768, 256)
-
+    both = project(512, 512)
+    queries[...] = both[:, :256]
+    att_q[...] = both[:, 256:]
+
+    o_step(1)
     for slot in range(2):
-        down, across = sums(slot)
-        q = rotated(queries, slot)
-        weight = jnp.where(ti >= tj, jnp.exp(jnp.where(ti >= tj, down - across, 0.0)), 0.0)
+        front, rear = rotated(queries, slot)
+        q = jnp.concatenate([front.astype(BF), rear.astype(BF)], axis=1)
         k = keys[pl.ds(ROWS * slot, ROWS)]
-        raw = dot(q.astype(BF), k, (((1,), (1,)), ((), ()))) * weight
+        raw = dot(q, k, (((1,), (1,)), ((), ()))) * inside[slot]
         scores[slot] = dot(raw.astype(BF), values[pl.ds(ROWS * slot, ROWS)])
-        queries[pl.ds(ROWS * slot, ROWS)] = (q * jnp.exp(down)).astype(BF)
-
+        queries[pl.ds(ROWS * slot, ROWS)] = jnp.concatenate(
+            [(front * grow[slot]).astype(BF), (rear * grow[slot]).astype(BF)], axis=1
+        )
+
+    o_step(2)
     arrived(rates.at[few], r_scan.at[0])
     arrived(came.at[few], r_scan.at[1])
 
@@ -409,14 +556,12 @@
 
     lax.fori_loop(0, 64, advance, jnp.zeros((16, 128), F32))
 
-    def give_back(k, _):
-        to = (me + k) % 64
-        send(back.at[to], prior.at[me], s_scan.at[2], r_scan.at[2], **place(to))
-        return 0
-
-    lax.fori_loop(1, 64, give_back, 0)
+    for k in offsets:
+        to, at = peer(k)
+        send(back.at[to], prior.at[me], s_scan.at[2], r_scan.at[2], **at)
     prior[me] = back[me]
 
+    o_step(3)
     @pl.when(me > 0)
     def _():
         arrived(lead, r_halo)
@@ -454,6 +599,7 @@
             def _(src=src, dst=dst, i=i):
                 send(src, dst, s_hid.at[2 + kind, i], r_hid.at[kind, x], x=to)
 
+    o_step(4)
     hand_over(1)
 
     arrived(prior.at[few], r_scan.at[2])
@@ -476,19 +622,38 @@
 
     hand_over(0)
 
-    for n in range(2):
-        for slot in range(2):
-            for half in range(2):
-                rows, cols = pl.ds(512 * half, 512), pl.ds(512 * slot, 512)
-                arrived(w_out.at[n, rows, cols], r_out.at[n, slot, half])
-    total = None
-    for kind in (1, 0):
-        for j in range(4):
-            arrived(heads.at[j, kind], r_hid.at[kind, j])
-        rows = jnp.concatenate([heads[j, kind] for j in range(4)], axis=1)
-        product = dot(rows, w_out[kind])
-        total = product if total is None else total + product
-    out_ref[...] = total.astype(BF)
+    for d in range(2):
+        for half in range(2):
+            for n in range(2):
+                rel = (2 * c + d + 3 - x) % 4
+                arrived(o_near.at[half, n, rel], r_out.at[half, n, rel])
+
+    @pl.when(at_home)
+    def _():
+        for half in range(2):
+            for n in range(2):
+                arrived(o_far.at[half, pl.ds(32 * n, 32), 3], r_own_far.at[half, n])
+
+    arrived(o_far.at[1 - c, :, three], r_o_mirror)
+
+    def product(kind, d):
+        rel = (2 * c + d + 3 - x) % 4
+        total = None
+        for half in range(2):
+            near_rows = o_near[half, kind, rel].reshape(256, 512)
+            far_rows = o_far[half, pl.ds(32 * kind, 32), rel].reshape(256, 512)
+            one = dot(heads[2 * half, kind], near_rows) + dot(heads[2 * half + 1, kind], far_rows)
+            total = one if total is None else total + one
+        return total
+
+    for j in range(4):
+        arrived(heads.at[j, 1], r_hid.at[1, j])
+    for d in range(2):
+        partial[d] = product(1, d)
+    for j in range(4):
+        arrived(heads.at[j, 0], r_hid.at[0, j])
+    for d in range(2):
+        out_ref[:, 512 * d : 512 * d + 512] = (partial[d] + product(0, d)).astype(BF)
 
     arrived(x_in.at[0], s_tok.at[0])
     arrived(tok, s_tok.at[2])
@@ -501,13 +666,16 @@
     @pl.when(jnp.logical_not(at_home))
     def _():
         arrived(tok, s_tok.at[1])
-        arrived(w_out.at[:, pl.ds(0, 512), pl.ds(0, 512)], s_small.at[5])
+        arrived(o_near.at[0, :, pl.ds(0, 2)], s_small.at[5])
 
     @pl.when(at_home)
     def _():
         arrived(own, s_small.at[0])
 
-    arrived(w_out.at[:, pl.ds(0, 768)], s_out)
+    arrived(o_near.at[0, :, three], s_out)
+    arrived(o_far.at[0, 0, three], s_slice)
+    arrived(o_far.at[0, few, three], s_o)
+    arrived(o_far.at[0, :, three], s_o_mirror)
     for i in range(2):
         mine = jnp.logical_and(at_home, x % 2 == i)
 
@@ -547,19 +715,8 @@
     ret_out,
     att_out,
 ):
-    kv = jnp.stack(
-        [jnp.concatenate([a[:, i : i + HD] for a in (att_key, att_value)], axis=1) for i in (0, HD)]
-    )
-    pack = jnp.concatenate(
-        [
-            log_decay[0][:, None, :],
-            ret_gain.reshape(2, 1, 256),
-            jnp.pad(sink_logits.reshape(2, 1, 4), ((0, 0), (0, 0), (0, 252))),
-            jnp.zeros((2, 5, 256), F32),
-        ],
-        axis=1,
-    )
-    inverse = (1.0 / 10000.0 ** (jnp.arange(128, dtype=F32) / 128)).reshape(1, 128)
+    steps = np.arange(128, dtype=np.float32) / np.float32(128)
+    inverse = jnp.asarray((np.float32(1) / np.float32(10000) ** steps).reshape(1, 128))
     vmem = pl.BlockSpec(memory_space=pltpu.VMEM)
     hbm = pl.BlockSpec(memory_space=pl.ANY)
     dma = pltpu.SemaphoreType.DMA
@@ -570,7 +727,19 @@
         pltpu.VMEM((64, 2, 16, COLS), BF),
         pltpu.VMEM((2, 8, 256), F32),
         pltpu.VMEM((2, 256, 256), F32),
-        pltpu.VMEM((2, 1024, 1024), BF),
+        pltpu.VMEM((2, 2, 4, 32, 8, 512), BF),
+        pltpu.VMEM((2, 64, 4, 8, 512), BF),
+        pltpu.VMEM((2, 32, 128), BF),
+        pltpu.VMEM((2, 256), F32),
+        pltpu.VMEM((1, 512), F32),
+        pltpu.VMEM((1, 8), F32),
+        pltpu.VMEM((2, 8, 256), F32),
+        pltpu.VMEM((1, D), F32),
+        pltpu.VMEM((1, 128), F32),
+        pltpu.VMEM((2, ROWS, ROWS), F32),
+        pltpu.VMEM((2, ROWS, 128), F32),
+        pltpu.VMEM((2, ROWS, 128), F32),
+        pltpu.VMEM((2, ROWS, 512), F32),
         pltpu.VMEM((ROWS, 128), F32),
         pltpu.VMEM((ROWS, 128), F32),
         pltpu.VMEM((2 * ROWS, 256), BF),
@@ -588,7 +757,7 @@
         pltpu.VMEM((64, 16, 128), BF),
         pltpu.VMEM((2, 2, ROWS, 256), BF),
         pltpu.VMEM((4, 2, ROWS, 256), BF),
-        dma((11,)),
+        dma((16,)),
         dma((3,)),
         dma((2, 2, CHUNKS)),
         dma((6,)),
@@ -607,12 +776,20 @@
         dma((4, 2)),
         dma((2, 4)),
         dma,
-        dma((2, 2, 2)),
+        dma((2, 2, 4)),
+        dma((2, 2)),
+        dma,
+        dma((3,)),
+        dma,
+        dma((8,)),
+        dma((2, 5, 2)),
+        dma,
+        dma,
     ]
     mixed = pl.pallas_call(
         layer_kernel,
-        out_shape=jax.ShapeDtypeStruct((ROWS, 1024), BF),
-        in_specs=[hbm] * 5 + [hbm, hbm, hbm, hbm, hbm, vmem, vmem],
+        out_shape=pltpu.VMEM((ROWS, 1024), BF),
+        in_specs=[hbm] * 15,
         out_specs=vmem,
         scratch_shapes=scratch,
         compiler_params=pltpu.CompilerParams(
@@ -624,11 +801,14 @@
         ret_value,
         ret_query,
         att_query,
-        kv,
-        pack,
+        att_key,
+        att_value,
+        log_decay[0],
+        ret_gain.reshape(1, 512),
+        sink_logits.reshape(1, 8),
         start_state[0],
-        ret_out,
-        att_out,
+        ret_out.reshape(64, 8, 512),
+        att_out.reshape(64, 8, 512),
         norm_gain.reshape(1, D),
         inverse,
     )

time: 104 us -> 85.6 us (0.82)
  Pallas kernels: 97.4 us -> 84.6 us
  local copies, waits for them, and re-layouts: 4.18 us -> 0.8 us
  other arithmetic: 1.94 us -> 0 us
    pallas_call x1, Pallas kernels: 97.4 us -> 84.6 us  [shards(): pl.pallas_call(layer_kernel, out_shape=pltpu.VMEM((ROWS, 1024), BF), in_s...]
    unnamed x11 -> x1, local copies, waits for them, and re-layouts: 3.87 us -> 0.8 us
where the time goes in v3:
time: 85.6 us; the launch traced here: 85.4 us
  Pallas kernels  84.6 us (99%)
    pallas_call x1, Pallas kernels, shards(): pl.pallas_call(layer_kernel, out_shape=pltpu.VMEM((ROWS, 1024), BF), in_s...  84.6 us

profile of v3, /device:TPU:1, one launch (start us, length us, event | category | flops | bytes accessed | tf_op | source)
XLA Modules:
  0.0 85.4 jit_solution(16862210102034777265)
XLA Ops:
  0.0 84.6 %shard_map.145 = bf16[256,1024]{1,0:T(8,128)(2,1)S(1)} custom-call(bf16[256,1024]{1,0:T(8,128)(2,1)} %bitcast.10, bf16[32,512]{1,0:T(8,128)(2,1)} %rk_ref.1, bf16[32,512]{1,0:T(8,128)(2,1)} %rv_ref.1, bf16[32,512]{1,0:T(8,128)(2,1)} %rq_ref.1, bf16[32,512]{1,0:T(8,128)(2,1)} %aq_ref.1, bf16[32,128]{1,0:T(8,128)(2,1)} %ak_ref.1, bf16[32,128]{1,0:T(8,128)(2,1)} %av_ref.1, ...), custom_call_target="tpu_custom_call" | custom-call | tf_op jit(solution)/shard_map/pallas_call | solution.py:789
  84.6 0.8 copy.17

commit v4 on v3

--- a/solution.py
+++ b/solution.py
@@ -84,6 +84,7 @@
     s_small,
     r_pack,
     r_start,
+    s_open,
     s_w,
     r_own,
     r_near,
@@ -96,6 +97,8 @@
     r_halo,
     s_hid,
     r_hid,
+    s_pass,
+    r_pass,
     s_out,
     r_out,
     r_own_far,
@@ -131,7 +134,10 @@
     barrier = pltpu.get_barrier_semaphore()
     friends = [{"x": (x + d) % 4, "c": h} for d in (1, 2, 3) for h in (0, 1)]
     friends += [{"c": 1 - c}]
-    friends += [along_first(k) for k in range(1, 8)] + [along_second(k) for k in (1, 7)]
+    for k in range(1, 8):
+        friends += [along_first(k), along_first(k) | {"c": home}]
+    for k in (1, 7):
+        friends += [along_second(k), along_second(k) | {"c": home}]
     for friend in friends:
         pl.semaphore_signal(barrier, inc=1, device_id=friend)
 
@@ -148,7 +154,7 @@
         (tok_ref, tok),
     )
     small = [
-        pltpu.make_async_copy(src, dst, s_local.at[8 + n]) for n, (src, dst) in enumerate(small)
+        pltpu.make_async_copy(src, dst, s_local.at[1 + n]) for n, (src, dst) in enumerate(small)
     ]
     loads = []
     for n, ref in enumerate((rk_ref, rv_ref, rq_ref, aq_ref)):
@@ -158,7 +164,7 @@
                 pltpu.make_async_copy(
                     ref.at[pl.ds(16 * half, 16), cols],
                     own.at[half, :, pl.ds(256 * n, 256)],
-                    s_local.at[2 * n + half],
+                    s_local.at[0],
                 )
             )
     for load in small[:2]:
@@ -185,18 +191,27 @@
 
     @pl.when(at_home)
     def _():
-        for load in loads:
-            load.wait()
+        arrived(own.at[:, :, pl.ds(0, 1024)], s_local.at[0])
         both = [jnp.where(odd == 0, kv_raw[n, :, :HD], kv_raw[n, :, HD:]) for n in range(2)]
         both = jnp.concatenate(both, axis=1)
         for half in range(2):
             w_all[me, half, :, 1024:COLS] = both[16 * half : 16 * half + 16]
 
     small[7].wait()
-    pl.semaphore_wait(barrier, len(friends))
+    pl.semaphore_wait(barrier, jnp.where(at_home, 34, 16))
 
     @pl.when(at_home)
     def _():
+        for k in (1, 7, 2, 6, 3, 5, 4):
+            for h in range(2):
+                ref = w_all.at[me, h]
+                to = {"z": (z + h * k) % 8, "y": (y + (1 - h) * k) % 8, "c": h}
+                send(ref, ref, s_open, r_near.at[8 - k], **to)
+        for direction, k in ((0, 1), (1, 7)):
+            for h in range(2):
+                ref = w_all.at[me, h]
+                to = {"z": (z + (1 - h) * k) % 8, "y": (y + h * k) % 8, "c": h}
+                send(ref, ref, s_open, r_far.at[direction, 0, 0], **to)
         send(own, own, s_small.at[0], r_own, c=1 - c)
 
     part = ROWS // CHUNKS
@@ -233,6 +248,48 @@
                 c=1 - c,
             )
 
+    three = pl.ds(0, 3)
+    first_at = c * z + (1 - c) * y
+    second_at = (1 - c) * z + c * y
+    line = second_at * 8 + first_at
+
+    @pl.when(line < 32)
+    def _():
+        for d in (1, 2, 3):
+            src = ro_ref.at[32 + line % 32]
+            send(src, o_far.at[c, line, 3 - d], s_slice, r_slice.at[3 - d], x=(x + d) % 4)
+
+    @pl.when(line >= 32)
+    def _():
+        for d in (1, 2, 3):
+            src = ao_ref.at[32 + line % 32]
+            send(src, o_far.at[c, line, 3 - d], s_slice, r_slice.at[3 - d], x=(x + d) % 4)
+
+    def o_block(ka):
+        return o_far.at[c, second_at * 8 + (first_at + ka) % 8, three]
+
+    def o_group(kb, g):
+        at = pl.multiple_of(((second_at + kb) % 8) * 8 + 4 * g, 4)
+        return o_far.at[c, pl.ds(at, 4), three]
+
+    def o_forward(ref, direction, kb, g):
+        send(ref, ref, s_o, r_o_far.at[direction, kb - 1, g], **along_second(7 if direction else 1))
+
+    def o_mirror(ref):
+        send(ref, ref, s_o_mirror, r_o_mirror, c=1 - c)
+
+    def o_step(kb):
+        for g in range(2):
+            for direction in range(2):
+                limit = limits(g)[direction]
+                if kb > limit:
+                    continue
+                ref = o_group(kb if direction else 8 - kb, g)
+                arrived(ref, r_o_far.at[direction, kb - 1, g])
+                if kb < limit:
+                    o_forward(ref, direction, kb + 1, g)
+                o_mirror(ref)
+
     for i in range(2):
         mine = jnp.logical_and(at_home, x % 2 == i)
 
@@ -274,21 +331,11 @@
     def mirror(ref):
         send(ref, ref, s_mirror, r_mirror, c=1 - c)
 
-    @pl.when(jnp.logical_not(at_home))
-    def _():
-        arrived(own, r_own)
-
-    for k in (1, 7, 2, 6, 3, 5, 4):
-        send(block(0, 0), block(0, 0), s_w, r_near.at[8 - k], **along_first(k))
-
     def limits(n):
         return (4, 3) if n % 2 == 0 else (3, 4)
 
     def forward(ref, direction, kb, n):
-        send(ref, ref, s_w, r_far.at[direction, kb, n], **along_second(7 if direction else 1))
-
-    forward(block(0, 0), 0, 1, 0)
-    forward(block(0, 0), 1, 1, 0)
+        send(ref, ref, s_w, r_far.at[direction, kb - 1, n], **along_second(7 if direction else 1))
 
     for n in range(1, 8):
         ka = STEPS[n]
@@ -335,18 +382,15 @@
             if kb > limit:
                 continue
             ref = block(STEPS[n], kb if direction else 8 - kb)
-            arrived(ref, r_far.at[direction, kb, n])
+            arrived(ref, r_far.at[direction, kb - 1, n])
             if kb < limit:
                 forward(ref, direction, kb + 1, n)
             mirror(ref)
 
     relay(0)
-    for n in range(4):
+    for n in range(8):
         ring(1, n)
     relay(1)
-    for n in range(4, 8):
-        ring(1, n)
-    relay(2)
 
     arrived(pack.at[0], r_pack.at[0])
     arrived(pack.at[1], r_pack.at[1])
@@ -371,40 +415,34 @@
         if n == 1:
             decays(0)
         if n == 3:
-            relay(3)
+            relay(2)
         if n == 5:
             decays(1)
-
-    first_at = c * z + (1 - c) * y
-    second_at = (1 - c) * z + c * y
-    line = second_at * 8 + first_at
-
-    @pl.when(line < 32)
-    def _():
-        for d in (1, 2, 3):
-            src = ro_ref.at[32 + line % 32]
-            send(src, o_far.at[c, line, 3 - d], s_slice, r_slice.at[3 - d], x=(x + d) % 4)
-
-    @pl.when(line >= 32)
-    def _():
-        for d in (1, 2, 3):
-            src = ao_ref.at[32 + line % 32]
-            send(src, o_far.at[c, line, 3 - d], s_slice, r_slice.at[3 - d], x=(x + d) % 4)
-
-    low, high, three = pl.ds(0, 32), pl.ds(32, 32), pl.ds(0, 3)
+    for n in range(8):
+        ring(3, n)
+        if n == 3:
+            relay(3)
+    for d in range(3):
+        arrived(o_far.at[c, line, d], r_slice.at[d])
+    for k in (4, 3, 5, 2, 6, 1, 7):
+        send(o_block(0), o_block(0), s_o, r_o_near.at[8 - k], **along_first(k))
+    for n in range(8):
+        ring(4, n)
+        norm_rows(near, n)
+    low, high = pl.ds(0, 32), pl.ds(32, 32)
     for n, ref in enumerate((ro_ref, ao_ref)):
         for d in (1, 2, 3):
             send(
                 ref.at[low],
                 o_near.at[c, n, 3 - d],
                 s_out,
-                r_out.at[c, n, 3 - d],
+                r_out.at[3 - d],
                 x=(x + d) % 4,
                 c=home,
             )
         pairs = (
-            (ref.at[low], o_near.at[c, n, 3], r_out.at[c, n, 3]),
-            (ref.at[high], o_far.at[c, pl.ds(32 * n, 32), 3], r_own_far.at[c, n]),
+            (ref.at[low], o_near.at[c, n, 3], r_out.at[3]),
+            (ref.at[high], o_far.at[c, pl.ds(32 * n, 32), 3], r_own_far),
         )
 
         @pl.when(at_home)
@@ -417,49 +455,14 @@
             for src, dst, sem in pairs:
                 send(src, dst, s_small.at[5], sem, c=1 - c)
 
-    def o_block(ka):
-        return o_far.at[c, second_at * 8 + (first_at + ka) % 8, three]
-
-    def o_group(kb, g):
-        at = pl.multiple_of(((second_at + kb) % 8) * 8 + 4 * g, 4)
-        return o_far.at[c, pl.ds(at, 4), three]
-
-    def o_forward(ref, direction, kb, g):
-        send(ref, ref, s_o, r_o_far.at[direction, kb, g], **along_second(7 if direction else 1))
-
-    def o_mirror(ref):
-        send(ref, ref, s_o_mirror, r_o_mirror, c=1 - c)
-
-    def o_step(kb):
-        for g in range(2):
-            for direction in range(2):
-                limit = limits(g)[direction]
-                if kb > limit:
-                    continue
-                ref = o_group(kb if direction else 8 - kb, g)
-                arrived(ref, r_o_far.at[direction, kb, g])
-                if kb < limit:
-                    o_forward(ref, direction, kb + 1, g)
-                o_mirror(ref)
-
     for n in range(8):
-        ring(3, n)
-        norm_rows(near, n)
-    for d in range(3):
-        arrived(o_far.at[c, line, d], r_slice.at[d])
-    for k in (4, 3, 5, 2, 6, 1, 7):
-        send(o_block(0), o_block(0), s_o, r_o_near.at[8 - k], **along_first(k))
-    for n in range(8):
-        ring(4, n)
         norm_rows(1 - near, n)
-    for k in range(1, 8):
-        arrived(o_block(k), r_o_near.at[k])
-    for g in range(2):
-        o_forward(o_group(0, g), 0, 1, g)
-        o_forward(o_group(0, g), 1, 1, g)
-        o_mirror(o_group(0, g))
     few = pl.ds(0, 63)
     arrived(w_all.at[few, 0], r_mirror)
+
+    @pl.when(jnp.logical_not(at_home))
+    def _():
+        arrived(own, r_own)
 
     def project(at, width):
         w = w_all[:, :, :, at : at + width].reshape(D, width)
@@ -498,6 +501,12 @@
                     slot, 16 * i : 16 * i + 16, 128 * half : 128 * half + 128
                 ].astype(BF)
 
+    for k in range(1, 8):
+        arrived(o_block(k), r_o_near.at[k])
+    for g in range(2):
+        o_forward(o_group(0, g), 0, 1, g)
+        o_forward(o_group(0, g), 1, 1, g)
+        o_mirror(o_group(0, g))
     def place(index):
         return {"z": index // 8, "y": index % 8}
 
@@ -535,7 +544,6 @@
     queries[...] = both[:, :256]
     att_q[...] = both[:, 256:]
 
-    o_step(1)
     for slot in range(2):
         front, rear = rotated(queries, slot)
         q = jnp.concatenate([front.astype(BF), rear.astype(BF)], axis=1)
@@ -546,7 +554,7 @@
             [(front * grow[slot]).astype(BF), (rear * grow[slot]).astype(BF)], axis=1
         )
 
-    o_step(2)
+    o_step(1)
     arrived(rates.at[few], r_scan.at[0])
     arrived(came.at[few], r_scan.at[1])
 
@@ -561,10 +569,11 @@
         send(back.at[to], prior.at[me], s_scan.at[2], r_scan.at[2], **at)
     prior[me] = back[me]
 
-    o_step(3)
+    o_step(2)
     @pl.when(me > 0)
     def _():
         arrived(lead, r_halo)
+
 
     qi = lax.broadcasted_iota(jnp.int32, (WINDOW, 2 * WINDOW), 0)
     ki = lax.broadcasted_iota(jnp.int32, (WINDOW, 2 * WINDOW), 1)
@@ -576,32 +585,49 @@
                 allowed = jnp.logical_and(allowed, ki >= jnp.where(me == 0, WINDOW, 0))
             kv = att_kv[slot, pl.ds(WINDOW * n, 2 * WINDOW)]
             rows = att_q[pl.ds(ROWS * slot + WINDOW * n, WINDOW)]
-            outs = []
-            for g in range(4):
-                score = dot(rows[:, HD * g : HD * g + HD], kv[:, :HD], (((1,), (1,)), ((), ())))
-                expo = jnp.exp(jnp.where(allowed, score * HD ** (-0.5), -1e30))
-                total = jnp.sum(expo, axis=-1, keepdims=True) + sink[:, g : g + 1]
-                outs.append(dot((expo / total).astype(BF), kv[:, HD:]))
+            heads_in = [rows[:, HD * g : HD * g + HD] for g in range(4)]
+            near_keys, near_values = kv[:, :HD], kv[:, HD:]
+            score = [dot(q, near_keys, (((1,), (1,)), ((), ()))) for q in heads_in]
+            expo = [jnp.exp(jnp.where(allowed, a * HD ** (-0.5), -1e30)) for a in score]
+            total = [
+                jnp.sum(e, axis=-1, keepdims=True) + sink[:, g : g + 1] for g, e in enumerate(expo)
+            ]
+            share = [(e * (1.0 / t)).astype(BF) for e, t in zip(expo, total)]
+            outs = [dot(p, near_values) for p in share]
             hidden[slot, 1, pl.ds(WINDOW * n, WINDOW)] = jnp.concatenate(outs, axis=1).astype(BF)
 
     def hand_over(kind):
         for i in range(2):
-            src = hidden.at[i, kind]
-            dst = heads.at[x, kind]
             to = 2 * c + i
-            send(src, dst, s_hid.at[kind, i], r_hid.at[kind, x], x=to, c=1 - c)
-
-            @pl.when(to == x)
-            def _(src=src, dst=dst):
-                pltpu.make_async_copy(src, dst, r_hid.at[kind, x]).start()
-
-            @pl.when(to != x)
-            def _(src=src, dst=dst, i=i):
-                send(src, dst, s_hid.at[2 + kind, i], r_hid.at[kind, x], x=to)
-
-    o_step(4)
+            for half in range(2):
+                rows = pl.ds(WINDOW * half, WINDOW)
+                src = hidden.at[i, kind, rows]
+                dst = heads.at[x, kind, rows]
+                here = jnp.logical_and(to == x, c == half)
+
+                @pl.when(here)
+                def _(src=src, dst=dst):
+                    pltpu.make_async_copy(src, dst, r_hid.at[kind, x]).start()
+
+                @pl.when(jnp.logical_not(here))
+                def _(src=src, dst=dst, half=half, i=i):
+                    send(src, dst, s_hid.at[kind, i, half], r_hid.at[kind, x], x=to, c=half)
+
+    def pass_on(kind):
+        rows = pl.ds(pl.multiple_of(WINDOW * c, WINDOW), WINDOW)
+        for j in range(4):
+            ref = heads.at[j, kind, rows]
+            arrived(ref, r_hid.at[kind, j])
+            send(ref, ref, s_pass, r_pass.at[kind, j], c=1 - c)
+
+    def passed(kind):
+        rows = pl.ds(pl.multiple_of(WINDOW * (1 - c), WINDOW), WINDOW)
+        for j in range(4):
+            arrived(heads.at[j, kind, rows], r_pass.at[kind, j])
+
     hand_over(1)
 
+    o_step(3)
     arrived(prior.at[few], r_scan.at[2])
     for slot in range(2):
         for i in range(16):
@@ -622,17 +648,14 @@
 
     hand_over(0)
 
+    o_step(4)
     for d in range(2):
-        for half in range(2):
-            for n in range(2):
-                rel = (2 * c + d + 3 - x) % 4
-                arrived(o_near.at[half, n, rel], r_out.at[half, n, rel])
+        rel = (2 * c + d + 3 - x) % 4
+        arrived(o_near.at[:, :, rel], r_out.at[rel])
 
     @pl.when(at_home)
     def _():
-        for half in range(2):
-            for n in range(2):
-                arrived(o_far.at[half, pl.ds(32 * n, 32), 3], r_own_far.at[half, n])
+        arrived(o_far.at[:, :, 3], r_own_far)
 
     arrived(o_far.at[1 - c, :, three], r_o_mirror)
 
@@ -646,19 +669,21 @@
             total = one if total is None else total + one
         return total
 
-    for j in range(4):
-        arrived(heads.at[j, 1], r_hid.at[1, j])
+    pass_on(1)
+    passed(1)
     for d in range(2):
         partial[d] = product(1, d)
-    for j in range(4):
-        arrived(heads.at[j, 0], r_hid.at[0, j])
+
+    pass_on(0)
+    passed(0)
     for d in range(2):
         out_ref[:, 512 * d : 512 * d + 512] = (partial[d] + product(0, d)).astype(BF)
 
     arrived(x_in.at[0], s_tok.at[0])
     arrived(tok, s_tok.at[2])
-    arrived(w_all.at[few, 0], s_w)
+    arrived(w_all.at[pl.ds(0, 54), 0], s_w)
     arrived(w_all.at[few, 0], s_mirror)
+    arrived(heads.at[pl.ds(0, 2)], s_pass)
     arrived(rates.at[few], s_scan.at[0])
     arrived(came.at[few], s_scan.at[1])
     arrived(prior.at[few], s_scan.at[2])
@@ -671,6 +696,7 @@
     @pl.when(at_home)
     def _():
         arrived(own, s_small.at[0])
+        arrived(w_all.at[pl.ds(0, 18), 0], s_open)
 
     arrived(o_near.at[0, :, three], s_out)
     arrived(o_far.at[0, 0, three], s_slice)
@@ -688,11 +714,13 @@
             arrived(start.at[i], s_small.at[3 + i])
 
         for kind in range(2):
-            arrived(hidden.at[i, kind], s_hid.at[kind, i])
-
-            @pl.when(2 * c + i != x)
-            def _(i=i, kind=kind):
-                arrived(hidden.at[i, kind], s_hid.at[2 + kind, i])
+            for half in range(2):
+                here = jnp.logical_and(2 * c + i == x, c == half)
+
+                @pl.when(jnp.logical_not(here))
+                def _(i=i, kind=kind, half=half):
+                    rows = pl.ds(WINDOW * half, WINDOW)
+                    arrived(hidden.at[i, kind, rows], s_hid.at[kind, i, half])
 
     @pl.when(me < 63)
     def _():
@@ -757,7 +785,7 @@
         pltpu.VMEM((64, 16, 128), BF),
         pltpu.VMEM((2, 2, ROWS, 256), BF),
         pltpu.VMEM((4, 2, ROWS, 256), BF),
-        dma((16,)),
+        dma((9,)),
         dma((3,)),
         dma((2, 2, CHUNKS)),
         dma((6,)),
@@ -765,24 +793,27 @@
         dma((2,)),
         dma,
         dma,
+        dma,
         dma((8,)),
-        dma((2, 5, 8)),
+        dma((2, 4, 8)),
         dma,
         dma,
         dma((3,)),
         dma((3,)),
         dma,
         dma,
-        dma((4, 2)),
+        dma((2, 2, 2)),
         dma((2, 4)),
         dma,
-        dma((2, 2, 4)),
-        dma((2, 2)),
+        dma((2, 4)),
+        dma,
+        dma((4,)),
+        dma,
         dma,
         dma((3,)),
         dma,
         dma((8,)),
-        dma((2, 5, 2)),
+        dma((2, 4, 2)),
         dma,
         dma,
     ]

time: 85.6 us -> 77.2 us (0.902)
  Pallas kernels: 84.6 us -> 76.2 us
    pallas_call x1, Pallas kernels: 84.6 us -> 76.2 us  [shards(): pl.pallas_call(layer_kernel, out_shape=pltpu.VMEM((ROWS, 1024), BF), in_s...]
where the time goes in v4:
time: 77.2 us; the launch traced here: 77 us
  Pallas kernels  76.2 us (99%)
  local copies, waits for them, and re-layouts  0.8 us (1%)
    pallas_call x1, Pallas kernels, shards(): pl.pallas_call(layer_kernel, out_shape=pltpu.VMEM((ROWS, 1024), BF), in_s...  76.2 us

profile of v4, /device:TPU:1, one launch (start us, length us, event | category | flops | bytes accessed | tf_op | source)
XLA Modules:
  0.0 77.0 jit_solution(4527547008078896965)
XLA Ops:
  0.0 76.2 %shard_map.145 = bf16[256,1024]{1,0:T(8,128)(2,1)S(1)} custom-call(bf16[256,1024]{1,0:T(8,128)(2,1)} %bitcast.10, bf16[32,512]{1,0:T(8,128)(2,1)} %rk_ref.1, bf16[32,512]{1,0:T(8,128)(2,1)} %rv_ref.1, bf16[32,512]{1,0:T(8,128)(2,1)} %rq_ref.1, bf16[32,512]{1,0:T(8,128)(2,1)} %aq_ref.1, bf16[32,128]{1,0:T(8,128)(2,1)} %ak_ref.1, bf16[32,128]{1,0:T(8,128)(2,1)} %av_ref.1, ...), custom_call_target="tpu_custom_call" | custom-call | tf_op jit(solution)/shard_map/pallas_call | solution.py:820
  76.2 0.8 %copy.17 = bf16[1,256,1024]{2,1,0:T(8,128)(2,1)} copy(bf16[1,256,1024]{2,1,0:T(8,128)(2,1)S(1)} %bitcast.9) | data formatting | bytes 1048576

commit v5 on v4

--- a/solution.py
+++ b/solution.py
@@ -104,6 +104,8 @@
     r_own_far,
     s_slice,
     r_slice,
+    s_relay,
+    s_o_near,
     s_o,
     r_o_near,
     r_o_far,
@@ -202,7 +204,7 @@
 
     @pl.when(at_home)
     def _():
-        for k in (1, 7, 2, 6, 3, 5, 4):
+        for k in (4, 3, 5, 2, 6, 1, 7):
             for h in range(2):
                 ref = w_all.at[me, h]
                 to = {"z": (z + h * k) % 8, "y": (y + (1 - h) * k) % 8, "c": h}
@@ -214,6 +216,105 @@
                 send(ref, ref, s_open, r_far.at[direction, 0, 0], **to)
         send(own, own, s_small.at[0], r_own, c=1 - c)
 
+    for i in range(2):
+        mine = jnp.logical_and(at_home, x % 2 == i)
+
+        @pl.when(mine)
+        def _(i=i):
+            pltpu.make_async_copy(pack_own.at[i], pack.at[i], r_pack.at[i]).start()
+
+        @pl.when(jnp.logical_not(mine))
+        def _(i=i):
+            send(
+                pack_own.at[i],
+                pack.at[x % 2],
+                s_small.at[1 + i],
+                r_pack.at[x % 2],
+                x=2 * c + i,
+                c=home,
+            )
+
+    piece = (
+        pl.ds(pl.multiple_of((me % 32) // 2 * 16, 16), 16),
+        pl.ds(pl.multiple_of(me % 2 * 128, 128), 128),
+    )
+    opens = x % 2 == me // 32
+    for i in range(2):
+        mine = jnp.logical_and(at_home, x % 2 == i)
+
+        @pl.when(jnp.logical_and(opens, mine))
+        def _(i=i):
+            pltpu.make_async_copy(start_ref.at[i, *piece], start, r_start).start()
+
+        @pl.when(jnp.logical_and(opens, jnp.logical_not(mine)))
+        def _(i=i):
+            send(
+                start_ref.at[i, *piece],
+                start,
+                s_small.at[3 + i],
+                r_start,
+                x=2 * c + i,
+                c=home,
+            )
+
+    three = pl.ds(0, 3)
+    first_at = c * z + (1 - c) * y
+    second_at = (1 - c) * z + c * y
+    holder = first_at < 4
+    line = second_at * 4 + first_at % 4
+
+    def slices(ref):
+        for d in (1, 2, 3):
+            src = ref.at[48 + line % 16]
+            send(src, o_far.at[c, line, 3 - d], s_slice, r_slice.at[3 - d], x=(x + d) % 4)
+
+    @pl.when(jnp.logical_and(holder, line < 16))
+    def _():
+        slices(ro_ref)
+
+    @pl.when(jnp.logical_and(holder, line >= 16))
+    def _():
+        slices(ao_ref)
+
+    def o_group(kb):
+        at = pl.multiple_of(((second_at + kb) % 8) * 4, 4)
+        return o_far.at[c, pl.ds(at, 4), three]
+
+    def o_forward(ref, direction, kb):
+        send(ref, ref, s_o, r_o_far.at[direction, kb - 1], **along_second(7 if direction else 1))
+
+    def o_mirror(ref):
+        send(ref, ref, s_o_mirror, r_o_mirror, c=1 - c)
+
+    def o_open():
+        @pl.when(holder)
+        def _():
+            for d in range(3):
+                arrived(o_far.at[c, line, d], r_slice.at[d])
+            ref = o_far.at[c, line, three]
+            for k in (4, 3, 5, 2, 6, 1, 7):
+                send(ref, ref, s_o_near, r_o_near.at[first_at % 4], **along_first(k))
+
+    def o_line():
+        for k in range(4):
+            @pl.when(first_at != k)
+            def _(k=k):
+                arrived(o_far.at[c, second_at * 4 + k, three], r_o_near.at[k])
+
+        o_forward(o_group(0), 0, 1)
+        o_forward(o_group(0), 1, 1)
+        o_mirror(o_group(0))
+
+    def o_step(kb):
+        for direction, limit in ((0, 4), (1, 3)):
+            if kb > limit:
+                continue
+            ref = o_group(kb if direction else 8 - kb)
+            arrived(ref, r_o_far.at[direction, kb - 1])
+            if kb < limit:
+                o_forward(ref, direction, kb + 1)
+            o_mirror(ref)
+
     part = ROWS // CHUNKS
 
     def token_rows(slot, half, q):
@@ -248,81 +349,6 @@
                 c=1 - c,
             )
 
-    three = pl.ds(0, 3)
-    first_at = c * z + (1 - c) * y
-    second_at = (1 - c) * z + c * y
-    line = second_at * 8 + first_at
-
-    @pl.when(line < 32)
-    def _():
-        for d in (1, 2, 3):
-            src = ro_ref.at[32 + line % 32]
-            send(src, o_far.at[c, line, 3 - d], s_slice, r_slice.at[3 - d], x=(x + d) % 4)
-
-    @pl.when(line >= 32)
-    def _():
-        for d in (1, 2, 3):
-            src = ao_ref.at[32 + line % 32]
-            send(src, o_far.at[c, line, 3 - d], s_slice, r_slice.at[3 - d], x=(x + d) % 4)
-
-    def o_block(ka):
-        return o_far.at[c, second_at * 8 + (first_at + ka) % 8, three]
-
-    def o_group(kb, g):
-        at = pl.multiple_of(((second_at + kb) % 8) * 8 + 4 * g, 4)
-        return o_far.at[c, pl.ds(at, 4), three]
-
-    def o_forward(ref, direction, kb, g):
-        send(ref, ref, s_o, r_o_far.at[direction, kb - 1, g], **along_second(7 if direction else 1))
-
-    def o_mirror(ref):
-        send(ref, ref, s_o_mirror, r_o_mirror, c=1 - c)
-
-    def o_step(kb):
-        for g in range(2):
-            for direction in range(2):
-                limit = limits(g)[direction]
-                if kb > limit:
-                    continue
-                ref = o_group(kb if direction else 8 - kb, g)
-                arrived(ref, r_o_far.at[direction, kb - 1, g])
-                if kb < limit:
-                    o_forward(ref, direction, kb + 1, g)
-                o_mirror(ref)
-
-    for i in range(2):
-        mine = jnp.logical_and(at_home, x % 2 == i)
-
-        @pl.when(mine)
-        def _(i=i):
-            pltpu.make_async_copy(pack_own.at[i], pack.at[i], r_pack.at[i]).start()
-
-        @pl.when(jnp.logical_not(mine))
-        def _(i=i):
-            send(
-                pack_own.at[i],
-                pack.at[x % 2],
-                s_small.at[1 + i],
-                r_pack.at[x % 2],
-                x=2 * c + i,
-                c=home,
-            )
-
-        @pl.when(jnp.logical_and(me == 0, mine))
-        def _(i=i):
-            pltpu.make_async_copy(start_ref.at[i], start.at[i], r_start.at[i]).start()
-
-        @pl.when(jnp.logical_and(me == 0, jnp.logical_not(mine)))
-        def _(i=i):
-            send(
-                start_ref.at[i],
-                start.at[x % 2],
-                s_small.at[3 + i],
-                r_start.at[x % 2],
-                x=2 * c + i,
-                c=home,
-            )
-
     def block(ka, kb):
         zz = (z + c * ka + (1 - c) * kb) % 8
         yy = (y + (1 - c) * ka + c * kb) % 8
@@ -336,61 +362,6 @@
 
     def forward(ref, direction, kb, n):
         send(ref, ref, s_w, r_far.at[direction, kb - 1, n], **along_second(7 if direction else 1))
-
-    for n in range(1, 8):
-        ka = STEPS[n]
-        ref = block(ka, 0)
-        arrived(ref, r_near.at[ka])
-        forward(ref, 0, 1, n)
-        forward(ref, 1, 1, n)
-        mirror(ref)
-
-    onward = at_home == (x % 2 == 0)
-    relay_half = jnp.where(onward, 1, 0)
-    relay_to = (x + jnp.where(onward, 3, 1)) % 4
-
-    def relay(q):
-        ref = token_rows(near, relay_half, q)
-        arrived(ref, r_tok.at[near, relay_half, q])
-        send(ref, ref, s_tok.at[2], r_tok.at[near, relay_half, q], x=relay_to)
-
-    def norm_rows(slot, t):
-        if t % 2 == 0:
-            q = t // 2
-
-            @pl.when(slot == near)
-            def _():
-                arrived(token_rows(near, 1 - relay_half, q), r_tok.at[near, 1 - relay_half, q])
-
-            @pl.when(slot != near)
-            def _():
-                for half in range(2):
-                    arrived(token_rows(1 - near, half, q), r_tok.at[1 - near, half, q])
-
-        rows = pl.ds(32 * t, 32)
-        a = x_in[slot, 0, rows].astype(F32)
-        b = x_in[slot, 1, rows].astype(F32)
-        total = jnp.sum(a * a, axis=-1, keepdims=True) + jnp.sum(b * b, axis=-1, keepdims=True)
-        scale = lax.rsqrt(total * (1.0 / D) + EPS)
-        to = pl.ds(pl.multiple_of(slot * ROWS + 32 * t, 32), 32)
-        normed[to, 0:1024] = (a * scale * gain[:, 0:1024]).astype(BF)
-        normed[to, 1024:2048] = (b * scale * gain[:, 1024:2048]).astype(BF)
-
-    def ring(kb, n):
-        for direction in range(2):
-            limit = limits(n)[direction]
-            if kb > limit:
-                continue
-            ref = block(STEPS[n], kb if direction else 8 - kb)
-            arrived(ref, r_far.at[direction, kb - 1, n])
-            if kb < limit:
-                forward(ref, direction, kb + 1, n)
-            mirror(ref)
-
-    relay(0)
-    for n in range(8):
-        ring(1, n)
-    relay(1)
 
     arrived(pack.at[0], r_pack.at[0])
     arrived(pack.at[1], r_pack.at[1])
@@ -410,51 +381,114 @@
         fall[slot] = jnp.broadcast_to(jnp.exp(last - down), (ROWS, 128))
         own_rate[slot] = jnp.broadcast_to(jnp.exp(last), (1, 128))
 
+    for n in range(1, 8):
+        ka = STEPS[n]
+        ref = block(ka, 0)
+        arrived(ref, r_near.at[ka])
+        forward(ref, 0, 1, n)
+        forward(ref, 1, 1, n)
+        mirror(ref)
+        if n == 1:
+            o_open()
+        if n == 2:
+            decays(0)
+        if n == 4:
+            decays(1)
+
+    onward = at_home == (x % 2 == 0)
+    relay_half = jnp.where(onward, 1, 0)
+    relay_to = (x + jnp.where(onward, 3, 1)) % 4
+
+    def relay(q):
+        ref = token_rows(near, relay_half, q)
+        arrived(ref, r_tok.at[near, relay_half, q])
+        send(ref, ref, s_tok.at[2], r_tok.at[near, relay_half, q], x=relay_to)
+
+    def norm_rows(slot, t):
+        if t % 2 == 0:
+            q = t // 2
+
+            @pl.when(slot == near)
+            def _():
+                arrived(token_rows(near, 1 - relay_half, q), r_tok.at[near, 1 - relay_half, q])
+
+            @pl.when(slot != near)
+            def _():
+                for half in range(2):
+                    arrived(token_rows(1 - near, half, q), r_tok.at[1 - near, half, q])
+
+        rows = pl.ds(32 * t, 32)
+        a = x_in[slot, 0, rows].astype(F32)
+        b = x_in[slot, 1, rows].astype(F32)
+        total = jnp.sum(a * a, axis=-1, keepdims=True) + jnp.sum(b * b, axis=-1, keepdims=True)
+        scale = lax.rsqrt(total * (1.0 / D) + EPS)
+        to = pl.ds(pl.multiple_of(slot * ROWS + 32 * t, 32), 32)
+        normed[to, 0:1024] = (a * scale * gain[:, 0:1024]).astype(BF)
+        normed[to, 1024:2048] = (b * scale * gain[:, 1024:2048]).astype(BF)
+
+    def ring(kb, n):
+        for direction in range(2):
+            limit = limits(n)[direction]
+            if kb > limit:
+                continue
+            ref = block(STEPS[n], kb if direction else 8 - kb)
+            arrived(ref, r_far.at[direction, kb - 1, n])
+            if kb < limit:
+                forward(ref, direction, kb + 1, n)
+            mirror(ref)
+
+    relay(0)
+    for n in range(8):
+        ring(1, n)
+    relay(1)
+
+    def send_along_x():
+        low, high = pl.ds(0, 48), pl.ds(48, 16)
+        for n, ref in enumerate((ro_ref, ao_ref)):
+            for d in (1, 3):
+                send(
+                    ref.at[low],
+                    o_near.at[c, n, 3 - d],
+                    s_out,
+                    r_out.at[3 - d, c, n],
+                    x=(x + d) % 4,
+                    c=home,
+                )
+            pairs = (
+                (ref.at[low], o_near.at[c, n, 3], r_out.at[3, c, n]),
+                (ref.at[high], o_far.at[c, pl.ds(16 * n, 16), 3], r_own_far),
+            )
+
+            @pl.when(at_home)
+            def _(pairs=pairs):
+                for src, dst, sem in pairs:
+                    pltpu.make_async_copy(src, dst, sem).start()
+
+            @pl.when(jnp.logical_not(at_home))
+            def _(pairs=pairs):
+                for src, dst, sem in pairs:
+                    send(src, dst, s_small.at[5], sem, c=1 - c)
+
+    def o_relay(n):
+        at = jnp.where(onward, 0, 2)
+        src = o_near.at[relay_half, n, at]
+        arrived(src, r_out.at[at, relay_half, n])
+        dst = o_near.at[relay_half, n, 1]
+        send(src, dst, s_relay, r_out.at[1, relay_half, n], x=relay_to)
+
     for n in range(8):
         ring(2, n)
-        if n == 1:
-            decays(0)
         if n == 3:
             relay(2)
-        if n == 5:
-            decays(1)
     for n in range(8):
         ring(3, n)
         if n == 3:
             relay(3)
-    for d in range(3):
-        arrived(o_far.at[c, line, d], r_slice.at[d])
-    for k in (4, 3, 5, 2, 6, 1, 7):
-        send(o_block(0), o_block(0), s_o, r_o_near.at[8 - k], **along_first(k))
+            send_along_x()
+    o_line()
     for n in range(8):
         ring(4, n)
         norm_rows(near, n)
-    low, high = pl.ds(0, 32), pl.ds(32, 32)
-    for n, ref in enumerate((ro_ref, ao_ref)):
-        for d in (1, 2, 3):
-            send(
-                ref.at[low],
-                o_near.at[c, n, 3 - d],
-                s_out,
-                r_out.at[3 - d],
-                x=(x + d) % 4,
-                c=home,
-            )
-        pairs = (
-            (ref.at[low], o_near.at[c, n, 3], r_out.at[3]),
-            (ref.at[high], o_far.at[c, pl.ds(32 * n, 32), 3], r_own_far),
-        )
-
-        @pl.when(at_home)
-        def _(pairs=pairs):
-            for src, dst, sem in pairs:
-                pltpu.make_async_copy(src, dst, sem).start()
-
-        @pl.when(jnp.logical_not(at_home))
-        def _(pairs=pairs):
-            for src, dst, sem in pairs:
-                send(src, dst, s_small.at[5], sem, c=1 - c)
-
     for n in range(8):
         norm_rows(1 - near, n)
     few = pl.ds(0, 63)
@@ -490,23 +524,13 @@
             [front.astype(BF), rear.astype(BF)], axis=1
         )
 
-        @pl.when(me == 0)
-        def _(slot=slot):
-            arrived(start.at[slot], r_start.at[slot])
-            state[slot] = state[slot] + own_rate[slot][:, 0:1] * start[slot]
-
         for i in range(16):
             for half in range(2):
                 pieces[slot * 32 + i * 2 + half] = state[
                     slot, 16 * i : 16 * i + 16, 128 * half : 128 * half + 128
                 ].astype(BF)
 
-    for k in range(1, 8):
-        arrived(o_block(k), r_o_near.at[k])
-    for g in range(2):
-        o_forward(o_group(0, g), 0, 1, g)
-        o_forward(o_group(0, g), 1, 1, g)
-        o_mirror(o_group(0, g))
+    o_step(1)
     def place(index):
         return {"z": index // 8, "y": index % 8}
 
@@ -544,6 +568,8 @@
     queries[...] = both[:, :256]
     att_q[...] = both[:, 256:]
 
+    o_step(2)
+    o_relay(0)
     for slot in range(2):
         front, rear = rotated(queries, slot)
         q = jnp.concatenate([front.astype(BF), rear.astype(BF)], axis=1)
@@ -554,7 +580,8 @@
             [(front * grow[slot]).astype(BF), (rear * grow[slot]).astype(BF)], axis=1
         )
 
-    o_step(1)
+    o_relay(1)
+    o_step(3)
     arrived(rates.at[few], r_scan.at[0])
     arrived(came.at[few], r_scan.at[1])
 
@@ -562,14 +589,14 @@
         back[k] = carried.astype(BF)
         return carried * rates[k] + came[k].astype(F32)
 
-    lax.fori_loop(0, 64, advance, jnp.zeros((16, 128), F32))
+    arrived(start, r_start)
+    lax.fori_loop(0, 64, advance, start[...])
 
     for k in offsets:
         to, at = peer(k)
         send(back.at[to], prior.at[me], s_scan.at[2], r_scan.at[2], **at)
     prior[me] = back[me]
 
-    o_step(2)
     @pl.when(me > 0)
     def _():
         arrived(lead, r_halo)
@@ -627,7 +654,7 @@
 
     hand_over(1)
 
-    o_step(3)
+    o_step(4)
     arrived(prior.at[few], r_scan.at[2])
     for slot in range(2):
         for i in range(16):
@@ -636,10 +663,6 @@
                     slot * 32 + i * 2 + half
                 ].astype(F32)
 
-        @pl.when(me == 0)
-        def _(slot=slot):
-            state[slot] = start[slot]
-
         raw = scores[slot] + dot(queries[pl.ds(ROWS * slot, ROWS)], state[slot].astype(BF))
         centred = raw - jnp.mean(raw, axis=-1, keepdims=True)
         variance = jnp.mean(centred * centred, axis=-1, keepdims=True)
@@ -648,10 +671,15 @@
 
     hand_over(0)
 
-    o_step(4)
     for d in range(2):
         rel = (2 * c + d + 3 - x) % 4
-        arrived(o_near.at[:, :, rel], r_out.at[rel])
+        for half in range(2):
+            relayed = jnp.logical_and(rel == jnp.where(onward, 0, 2), relay_half == half)
+
+            @pl.when(jnp.logical_not(relayed))
+            def _(rel=rel, half=half):
+                for n in range(2):
+                    arrived(o_near.at[half, n, rel], r_out.at[rel, half, n])
 
     @pl.when(at_home)
     def _():
@@ -663,9 +691,11 @@
         rel = (2 * c + d + 3 - x) % 4
         total = None
         for half in range(2):
-            near_rows = o_near[half, kind, rel].reshape(256, 512)
-            far_rows = o_far[half, pl.ds(32 * kind, 32), rel].reshape(256, 512)
-            one = dot(heads[2 * half, kind], near_rows) + dot(heads[2 * half + 1, kind], far_rows)
+            even = o_near[half, kind, rel, 0:32].reshape(256, 512)
+            front = o_near[half, kind, rel, 32:48].reshape(128, 512)
+            rear = o_far[half, pl.ds(16 * kind, 16), rel].reshape(128, 512)
+            odd_rows = jnp.concatenate([front, rear], axis=0)
+            one = dot(heads[2 * half, kind], even) + dot(heads[2 * half + 1, kind], odd_rows)
             total = one if total is None else total + one
         return total
 
@@ -691,16 +721,22 @@
     @pl.when(jnp.logical_not(at_home))
     def _():
         arrived(tok, s_tok.at[1])
-        arrived(o_near.at[0, :, pl.ds(0, 2)], s_small.at[5])
+        arrived(o_far.at[:, :, pl.ds(0, 2)], s_small.at[5])
 
     @pl.when(at_home)
     def _():
         arrived(own, s_small.at[0])
         arrived(w_all.at[pl.ds(0, 18), 0], s_open)
 
-    arrived(o_near.at[0, :, three], s_out)
-    arrived(o_far.at[0, 0, three], s_slice)
-    arrived(o_far.at[0, few, three], s_o)
+    arrived(o_near.at[0, :, pl.ds(0, 2)], s_out)
+    arrived(o_near.at[0, :, 1], s_relay)
+    arrived(o_far.at[0, pl.ds(0, 28), three], s_o)
+
+    @pl.when(holder)
+    def _():
+        arrived(o_far.at[0, 0, three], s_slice)
+        arrived(o_far.at[0, pl.ds(0, 7), three], s_o_near)
+
     arrived(o_far.at[0, :, three], s_o_mirror)
     for i in range(2):
         mine = jnp.logical_and(at_home, x % 2 == i)
@@ -709,9 +745,9 @@
         def _(i=i):
             arrived(pack.at[i], s_small.at[1 + i])
 
-        @pl.when(jnp.logical_and(me == 0, jnp.logical_not(mine)))
+        @pl.when(jnp.logical_and(opens, jnp.logical_not(mine)))
         def _(i=i):
-            arrived(start.at[i], s_small.at[3 + i])
+            arrived(start, s_small.at[3 + i])
 
         for kind in range(2):
             for half in range(2):
@@ -754,9 +790,9 @@
         pltpu.VMEM((2 * ROWS, D), BF),
         pltpu.VMEM((64, 2, 16, COLS), BF),
         pltpu.VMEM((2, 8, 256), F32),
-        pltpu.VMEM((2, 256, 256), F32),
-        pltpu.VMEM((2, 2, 4, 32, 8, 512), BF),
-        pltpu.VMEM((2, 64, 4, 8, 512), BF),
+        pltpu.VMEM((16, 128), F32),
+        pltpu.VMEM((2, 2, 4, 48, 8, 512), BF),
+        pltpu.VMEM((2, 32, 4, 8, 512), BF),
         pltpu.VMEM((2, 32, 128), BF),
         pltpu.VMEM((2, 256), F32),
         pltpu.VMEM((1, 512), F32),
@@ -790,7 +826,7 @@
         dma((2, 2, CHUNKS)),
         dma((6,)),
         dma((2,)),
-        dma((2,)),
+        dma,
         dma,
         dma,
         dma,
@@ -807,13 +843,15 @@
         dma,
         dma((2, 4)),
         dma,
+        dma((4, 2, 2)),
+        dma,
+        dma,
+        dma((3,)),
+        dma,
+        dma,
+        dma,
         dma((4,)),
-        dma,
-        dma,
-        dma((3,)),
-        dma,
-        dma((8,)),
-        dma((2, 4, 2)),
+        dma((2, 4)),
         dma,
         dma,
     ]

time: 77.2 us -> 72.7 us (0.942)
  Pallas kernels: 76.2 us -> 71.7 us
    pallas_call x1, Pallas kernels: 76.2 us -> 71.7 us  [shards(): pl.pallas_call(layer_kernel, out_shape=pltpu.VMEM((ROWS, 1024), BF), in_s...]
where the time goes in v5:
time: 72.7 us; the launch traced here: 72.5 us
  Pallas kernels  71.7 us (99%)
  local copies, waits for them, and re-layouts  0.8 us (1%)
    pallas_call x1, Pallas kernels, shards(): pl.pallas_call(layer_kernel, out_shape=pltpu.VMEM((ROWS, 1024), BF), in_s...  71.7 us

profile of v5, /device:TPU:1, one launch (start us, length us, event | category | flops | bytes accessed | tf_op | source)
XLA Modules:
  0.0 72.5 jit_solution(15949096122127471333)
XLA Ops:
  0.0 71.7 %shard_map.145 = bf16[256,1024]{1,0:T(8,128)(2,1)S(1)} custom-call(bf16[256,1024]{1,0:T(8,128)(2,1)} %bitcast.10, bf16[32,512]{1,0:T(8,128)(2,1)} %rk_ref.1, bf16[32,512]{1,0:T(8,128)(2,1)} %rv_ref.1, bf16[32,512]{1,0:T(8,128)(2,1)} %rq_ref.1, bf16[32,512]{1,0:T(8,128)(2,1)} %aq_ref.1, bf16[32,128]{1,0:T(8,128)(2,1)} %ak_ref.1, bf16[32,128]{1,0:T(8,128)(2,1)} %av_ref.1, ...), custom_call_target="tpu_custom_call" | custom-call | tf_op jit(solution)/shard_map/pallas_call | solution.py:858
  71.7 0.8 %copy.17 = bf16[1,256,1024]{2,1,0:T(8,128)(2,1)} copy(bf16[1,256,1024]{2,1,0:T(8,128)(2,1)S(1)} %bitcast.9) | data formatting | bytes 1048576

commit v6 on v5

--- a/solution.py
+++ b/solution.py
@@ -235,10 +235,11 @@
             )
 
     piece = (
-        pl.ds(pl.multiple_of((me % 32) // 2 * 16, 16), 16),
-        pl.ds(pl.multiple_of(me % 2 * 128, 128), 128),
+        pl.ds(pl.multiple_of(me // 4 * 16, 16), 16),
+        pl.ds(pl.multiple_of(me // 2 % 2 * 128, 128), 128),
     )
-    opens = x % 2 == me // 32
+    colour = (z + y) % 2
+    opens = x % 2 == colour
     for i in range(2):
         mine = jnp.logical_and(at_home, x % 2 == i)
 
@@ -485,11 +486,15 @@
         if n == 3:
             relay(3)
             send_along_x()
+        if n >= 4:
+            norm_rows(near, 2 * n - 8)
+            norm_rows(near, 2 * n - 7)
     o_line()
     for n in range(8):
         ring(4, n)
-        norm_rows(near, n)
-    for n in range(8):
+        if n < 6:
+            norm_rows(1 - near, n)
+    for n in (6, 7):
         norm_rows(1 - near, n)
     few = pl.ds(0, 63)
     arrived(w_all.at[few, 0], r_mirror)
@@ -537,20 +542,35 @@
     def reach(k):
         return min(k // 8, 8 - k // 8) + min(k % 8, 8 - k % 8)
 
-    offsets = sorted(range(1, 64), key=lambda k: (-reach(k), k))
-
-    def peer(k):
-        zz, yy = (z + k // 8) % 8, (y + k % 8) % 8
-        return zz * 8 + yy, {"z": zz, "y": yy}
-
-    for k in offsets:
-        to, at = peer(k)
-        send(pieces.at[to], came.at[me], s_scan.at[1], r_scan.at[1], **at)
-    for k in offsets:
-        to, at = peer(k)
-        send(own_rate.at[to // 32], rates.at[me], s_scan.at[0], r_scan.at[0], **at)
-    came[me] = pieces[me]
-    rates[me] = own_rate[me // 32]
+    offsets = sorted(
+        (8 * i + j for i in range(8) for j in range(8) if (i + j) % 2 == 0),
+        key=lambda k: (-reach(k), k),
+    )
+
+    def everyone(shade, visit):
+        shift = (colour + shade) % 2
+        for k in offsets:
+            zz, yy = (z + k // 8) % 8, (y + k % 8 + shift) % 8
+            to, at = zz * 8 + yy, {"z": zz, "y": yy}
+            if k > 0:
+                visit(to, at)
+            else:
+                pl.when(shift == 1)(lambda to=to, at=at: visit(to, at))
+
+    for shade in range(2):
+
+        def give(to, at, shade=shade):
+            ref = pieces.at[32 * shade + to // 2]
+            send(ref, came.at[me], s_scan.at[1], r_scan.at[1], **at)
+
+        def tell(to, at, shade=shade):
+            send(own_rate.at[shade], rates.at[me], s_scan.at[0], r_scan.at[0], **at)
+
+        everyone(shade, give)
+        everyone(shade, tell)
+    mine_at = 32 * colour + me // 2
+    came[me] = pieces[mine_at]
+    rates[me] = own_rate[colour]
 
     att_kv[:, pl.ds(WINDOW, ROWS)] = project(1024, 128).reshape(2, ROWS, 128)
     tail = att_kv.at[:, pl.ds(ROWS, WINDOW)]
@@ -592,11 +612,14 @@
     arrived(start, r_start)
     lax.fori_loop(0, 64, advance, start[...])
 
-    for k in offsets:
-        to, at = peer(k)
-        send(back.at[to], prior.at[me], s_scan.at[2], r_scan.at[2], **at)
-    prior[me] = back[me]
-
+    for shade in range(2):
+        everyone(
+            shade,
+            lambda to, at: send(
+                back.at[to], prior.at[mine_at], s_scan.at[2], r_scan.at[2], **at
+            ),
+        )
+    prior[mine_at] = back[me]
     @pl.when(me > 0)
     def _():
         arrived(lead, r_halo)

time: 72.7 us -> 72 us (level)
  no operation moved by 1% of the time
where the time goes in v6:
time: 72 us; the launch traced here: 71.9 us
  Pallas kernels  71.1 us (99%)
  local copies, waits for them, and re-layouts  0.8 us (1%)
    pallas_call x1, Pallas kernels, shards(): pl.pallas_call(layer_kernel, out_shape=pltpu.VMEM((ROWS, 1024), BF), in_s...  71.1 us

profile of v6, /device:TPU:1, one launch (start us, length us, event | category | flops | bytes accessed | tf_op | source)
XLA Modules:
  0.0 71.9 jit_solution(13055830197055263819)
XLA Ops:
  0.0 71.1 %shard_map.145 = bf16[256,1024]{1,0:T(8,128)(2,1)S(1)} custom-call(bf16[256,1024]{1,0:T(8,128)(2,1)} %bitcast.10, bf16[32,512]{1,0:T(8,128)(2,1)} %rk_ref.1, bf16[32,512]{1,0:T(8,128)(2,1)} %rv_ref.1, bf16[32,512]{1,0:T(8,128)(2,1)} %rq_ref.1, bf16[32,512]{1,0:T(8,128)(2,1)} %aq_ref.1, bf16[32,128]{1,0:T(8,128)(2,1)} %ak_ref.1, bf16[32,128]{1,0:T(8,128)(2,1)} %av_ref.1, ...), custom_call_target="tpu_custom_call" | custom-call | tf_op jit(solution)/shard_map/pallas_call | solution.py:881
  71.1 0.8 %copy.17 = bf16[1,256,1024]{2,1,0:T(8,128)(2,1)} copy(bf16[1,256,1024]{2,1,0:T(8,128)(2,1)S(1)} %bitcast.9) | data formatting | bytes 1048576

commit v7 on v6

--- a/solution.py
+++ b/solution.py
@@ -642,7 +642,7 @@
             total = [
                 jnp.sum(e, axis=-1, keepdims=True) + sink[:, g : g + 1] for g, e in enumerate(expo)
             ]
-            share = [(e * (1.0 / t)).astype(BF) for e, t in zip(expo, total)]
+            share = [(e * (1.0 / (t * 0.0625)) * 0.0625).astype(BF) for e, t in zip(expo, total)]
             outs = [dot(p, near_values) for p in share]
             hidden[slot, 1, pl.ds(WINDOW * n, WINDOW)] = jnp.concatenate(outs, axis=1).astype(BF)
 

time: 72 us -> 72 us (level)
  no operation moved by 1% of the time
where the time goes in v7:
time: 72 us; the launch traced here: 71.9 us
  Pallas kernels  71.1 us (99%)
  local copies, waits for them, and re-layouts  0.8 us (1%)
    pallas_call x1, Pallas kernels, shards(): pl.pallas_call(layer_kernel, out_shape=pltpu.VMEM((ROWS, 1024), BF), in_s...  71.1 us

profile of v7, /device:TPU:1, one launch (start us, length us, event | category | flops | bytes accessed | tf_op | source)
XLA Modules:
  0.0 71.9 jit_solution(7401846715426347027)
XLA Ops:
  0.0 71.1 %shard_map.145 = bf16[256,1024]{1,0:T(8,128)(2,1)S(1)} custom-call(bf16[256,1024]{1,0:T(8,128)(2,1)} %bitcast.10, bf16[32,512]{1,0:T(8,128)(2,1)} %rk_ref.1, bf16[32,512]{1,0:T(8,128)(2,1)} %rv_ref.1, bf16[32,512]{1,0:T(8,128)(2,1)} %rq_ref.1, bf16[32,512]{1,0:T(8,128)(2,1)} %aq_ref.1, bf16[32,128]{1,0:T(8,128)(2,1)} %ak_ref.1, bf16[32,128]{1,0:T(8,128)(2,1)} %av_ref.1, ...), custom_call_target="tpu_custom_call" | custom-call | tf_op jit(solution)/shard_map/pallas_call | solution.py:881
  71.1 0.8 %copy.17 = bf16[1,256,1024]{2,1,0:T(8,128)(2,1)} copy(bf16[1,256,1024]{2,1,0:T(8,128)(2,1)S(1)} %bitcast.9) | data formatting | bytes 1048576
